TPU v7x, 32 devices: a whole 2x2x4 slice. The times are simulated.
32 devices in a mesh: fs: 8 (over z, y), tp: 4 (over x, core).
Axes of the slice: x: 2, y: 2, z: 4, core: 2. Of those that a mesh axis runs over, the one named last changes fastest.
Arguments:
- prompt_tokens: bfloat16 [4, 128, 4096], P('tp'), may hold values from -6 to 6
- trained_up: float32 [4096, 16384], P('fs', 'tp'), may hold values from -0.09375 to 0.09375
- trained_down: float32 [16384, 4096], P('fs', 'tp'), may hold values from -0.046875 to 0.046875
- pre_gain: float32 [4096], P('fs'), may hold values from 0.1 to 1.9
- post_gain: float32 [4096], replicated, may hold values from 0.1 to 1.9
Outputs:
- layer_out: bfloat16 [4, 128, 4096], P('tp', 'fs')
- sampler_up: bfloat16 [4096, 16384], P(None, 'fs')
- sampler_down: bfloat16 [16384, 4096], P('fs')
All inputs are finite; a program needn't handle non-finite values.
Results may differ from a plain program's by a relative error of at most 0.0081.
Values may be sent and summed in bfloat16 or wider, within the bound.
A program may use at most 128 MiB of HBM per device.

v0:
```python
import functools

import jax
import jax.numpy as jnp
from jax import lax
from jax.experimental import pallas as pl
from jax.experimental.pallas import tpu as pltpu
from jax.sharding import PartitionSpec as P

MESH = pl.DeviceIdType.MESH
EPS = 1e-06


def remote(src, dst, send_sem, recv_sem, device):
    return pltpu.make_async_remote_copy(
        src_ref=src, dst_ref=dst, send_sem=send_sem, recv_sem=recv_sem, device_id=device, device_id_type=MESH
    )


def greet(device):
    pl.semaphore_signal(pltpu.get_barrier_semaphore(), inc=1, device_id=device, device_id_type=MESH)


def loop(count, body):
    lax.fori_loop(0, count, lambda i, c: (body(i), c)[1], 0)


def spread_kernel(
    n_fs, n_tp, n_r,
    up, down, tokens, gup, gdown, parts, held_up, held_down, xup, normed, upward, hidden,
    xs, xr, ps, pr, ws, wr, ns, nr, us, ls, ds, dr, vs, vr,
):
    f, t = lax.axis_index("fs"), lax.axis_index("tp")
    far = lax.rem(t + n_tp // 2, n_tp)
    near = t + 1 - 2 * lax.rem(t, 2)
    near_far = lax.rem(near + n_tp // 2, n_tp)
    m = n_fs // n_tp
    rows, width = up.shape[0], up.shape[1] // m
    part = rows // n_r
    d_rows, d_width = down.shape
    d_part = d_rows // n_r
    pieces = m * n_r
    block_of_f = f // m
    active = lax.rem(lax.rem(block_of_f, 2) + lax.rem(t, 2), 2) == 0

    def piece_at(r, j):
        return (
            pl.ds(pl.multiple_of(r * part, part), part),
            pl.ds(pl.multiple_of(j * width, width), width),
        )

    def piece(ref, k):
        return ref.at[piece_at(k // m, lax.rem(k, m))]

    def rows_of(source, r):
        return pl.ds(pl.multiple_of(source * rows + r * part, part), part)

    def landed(source, r):
        return held_up.at[rows_of(source, r)]

    def x_copy(k):
        return remote(piece(up, k), piece(xup, k), xs.at[k], xr.at[k], {"tp": far})

    def owner(phase, k):
        return (t if phase == 0 else far) * m + lax.rem(k, m)

    def peer_copy(phase, k):
        held = up if phase == 0 else xup
        return remote(piece(held, k), landed(f, k // m), ps.at[phase, k], pr.at[f, k // m], {"fs": owner(phase, k)})

    def start_peer(phase, k):
        @pl.when(owner(phase, k) != f)
        def _():
            peer_copy(phase, k).start()

    def end_peer(phase, k):
        @pl.when(owner(phase, k) != f)
        def _():
            peer_copy(phase, k).wait_send()

    def d_rows_of(q):
        return pl.ds(pl.multiple_of(q * d_part, d_part), d_part)

    def columns(which):
        return pl.ds(pl.multiple_of(which * d_width, d_width), d_width)

    def block(q, which):
        return held_down.at[which, d_rows_of(q)]

    def d_copy(q):
        return remote(down.at[d_rows_of(q)], block(q, t), ds.at[q], dr.at[q], {"tp": far})

    def d_pass(q, which):
        return remote(block(q, which), block(q, which), vs.at[q], vr.at[q], {"tp": near})

    def d_put(q, which):
        pltpu.make_async_copy(block(q, which), gdown.at[d_rows_of(q), columns(which)], ls).start()

    def share(src, source, r):
        return remote(src, landed(source, r), ws.at[source, r], wr.at[source, r], {"tp": near})

    def put(src, source, r):
        pltpu.make_async_copy(src, gup.at[rows_of(source, r)], us).start()

    loop(n_fs - 1, lambda i: greet({"fs": lax.rem(f + 1 + i, n_fs)}))
    greet({"tp": far})
    greet({"tp": near})
    pl.semaphore_wait(pltpu.get_barrier_semaphore(), n_fs + 1)

    loop(pieces, lambda k: x_copy(k).start())
    loop(pieces, lambda k: start_peer(0, k))
    to_near = remote(down, held_down.at[t], ns, nr, {"tp": near})
    to_near.start()
    pltpu.make_async_copy(down, gdown.at[:, columns(t)], ls).start()

    flat = tokens[...].astype(jnp.float32)
    scaled = (flat * lax.rsqrt(jnp.mean(flat * flat, axis=-1, keepdims=True) + EPS)).astype(jnp.bfloat16)
    for i in range(n_fs * n_r):
        normed[i] = scaled[:, i * part : (i + 1) * part]
    upward[...] = jnp.zeros_like(upward)

    def keep_down(q):
        held_down[t, d_rows_of(q)] = down[d_rows_of(q)]

    loop(n_r, keep_down)

    def pass_on(k):
        @pl.when(k == pieces - 1)
        def _():
            loop(n_r, lambda q: d_copy(q).start())

        x_copy(k).wait_recv()
        start_peer(1, k)

    loop(pieces, pass_on)

    def gather(r):
        def one(source):
            def keep_own(held):
                src = held.at[piece_at(r, lax.rem(f, m))]
                share(src, source, r).start()
                put(src, source, r)
                held_up[rows_of(source, r)] = held[piece_at(r, lax.rem(f, m))]

            @pl.when(jnp.logical_and(active, source == f))
            def _():
                @pl.when(block_of_f == t)
                def _():
                    keep_own(up)

                @pl.when(block_of_f != t)
                def _():
                    keep_own(xup)

            @pl.when(jnp.logical_and(active, source != f))
            def _():
                remote(landed(source, r), landed(source, r), ws.at[source, r], pr.at[source, r], {"tp": near}).wait_recv()
                share(landed(source, r), source, r).start()
                put(landed(source, r), source, r)

            @pl.when(jnp.logical_not(active))
            def _():
                share(landed(source, r), source, r).wait_recv()
                put(landed(source, r), source, r)

            upward[...] += jnp.dot(
                normed[source * n_r + r], held_up[rows_of(source, r)], preferred_element_type=jnp.float32
            )

        loop(n_fs, one)
        remote(block(r, far), block(r, far), ds.at[r], dr.at[r], {"tp": far}).wait_recv()
        d_pass(r, far).start()
        d_put(r, far)
        d_pass(r, near_far).wait_recv()
        d_put(r, near_far)

    loop(n_r, gather)
    remote(held_down.at[near], held_down.at[near], ns, nr, {"tp": near}).wait_recv()
    pltpu.make_async_copy(held_down.at[near], gdown.at[:, columns(near)], ls).start()

    hidden[...] = jnp.square(jnp.maximum(upward[...], 0.0)).astype(jnp.bfloat16)
    tile = min(d_width, 256)
    per_block = d_width // tile

    def finish(i):
        b, j = i // per_block, lax.rem(i, per_block)
        parts[:, pl.ds(pl.multiple_of(i * tile, tile), tile)] = jnp.dot(
            hidden[...],
            held_down[b, :, pl.ds(pl.multiple_of(j * tile, tile), tile)],
            preferred_element_type=jnp.float32,
        ).astype(parts.dtype)

    loop(n_tp * per_block, finish)

    def ended(i):
        @pl.when(active)
        def _():
            source, r = i // n_r, lax.rem(i, n_r)
            share(landed(source, r), source, r).wait_send()

    loop(n_fs * n_r, ended)
    to_near.wait_send()

    def ended_down(q):
        d_copy(q).wait_send()
        d_pass(q, far).wait_send()

    loop(n_r, ended_down)

    def ended_pieces(k):
        x_copy(k).wait_send()
        end_peer(0, k)
        end_peer(1, k)

    loop(pieces, ended_pieces)
    pltpu.make_async_copy(held_up, gup, us).wait()
    pltpu.make_async_copy(gdown, gdown, ls).wait()


def copy_kernel(up, down, up_out, down_out):
    up_out[...] = up[...]
    down_out[...] = down[...]


def sum_kernel(n_fs, parts, gain, out, land, ss, rs):
    f = lax.axis_index("fs")

    def peer_of(i):
        return lax.rem(f + 1 + i, n_fs)

    loop(n_fs - 1, lambda i: greet({"fs": peer_of(i)}))
    pl.semaphore_wait(pltpu.get_barrier_semaphore(), n_fs - 1)

    def send(i):
        return remote(parts.at[peer_of(i)], land.at[f], ss.at[i], rs.at[f], {"fs": peer_of(i)})

    loop(n_fs - 1, lambda i: send(i).start())

    def add(i, total):
        source = peer_of(i)
        remote(land.at[source], land.at[source], ss.at[i], rs.at[source], {"fs": source}).wait_recv()
        return total + land[source].astype(jnp.float32)

    summed = lax.fori_loop(0, n_fs - 1, add, parts[f].astype(jnp.float32))
    scale = lax.rsqrt(jnp.mean(summed * summed, axis=-1, keepdims=True) + EPS)
    out[...] = (summed * scale * gain[...]).astype(out.dtype)
    loop(n_fs - 1, lambda i: send(i).wait_send())


def on_device(n_fs, n_tp, prompt_tokens, trained_up, trained_down, pre_gain, post_gain):
    bf16 = jnp.bfloat16
    up = (pre_gain[:, None] * trained_up).astype(bf16)
    down = trained_down.astype(bf16)
    rows, cols = up.shape
    d_rows, d_cols = down.shape
    tokens, width = prompt_tokens.shape[1:]
    m = n_fs // n_tp
    owned = cols // m
    n_r = max(1, rows // 128)
    pieces = m * n_r
    anywhere = pl.BlockSpec(memory_space=pl.ANY)
    vmem = pl.BlockSpec(memory_space=pltpu.VMEM)
    dma = pltpu.SemaphoreType.DMA
    gup, gdown, parts = pl.pallas_call(
        functools.partial(spread_kernel, n_fs, n_tp, n_r),
        out_shape=(
            jax.ShapeDtypeStruct((n_fs * rows, owned), bf16),
            jax.ShapeDtypeStruct((d_rows, n_tp * d_cols), bf16),
            jax.ShapeDtypeStruct((tokens, width), bf16),
        ),
        in_specs=[vmem, vmem, vmem],
        out_specs=(anywhere, anywhere, vmem),
        scratch_shapes=[
            pltpu.VMEM((n_fs * rows, owned), bf16),
            pltpu.VMEM((n_tp, d_rows, d_cols), bf16),
            pltpu.VMEM(up.shape, bf16),
            pltpu.VMEM((n_fs * n_r, tokens, rows // n_r), bf16),
            pltpu.VMEM((tokens, owned), jnp.float32),
            pltpu.VMEM((tokens, owned), bf16),
            dma((pieces,)), dma((pieces,)),
            dma((2, pieces)), dma((n_fs, n_r)),
            dma((n_fs, n_r)), dma((n_fs, n_r)),
            dma, dma, dma, dma,
            dma((n_r,)), dma((n_r,)),
            dma((n_r,)), dma((n_r,)),
        ],
        compiler_params=pltpu.CompilerParams(collective_id=0, has_side_effects=True, vmem_limit_bytes=64000000),
    )(up, down, prompt_tokens[0])

    steps = 8
    blocks = [
        pl.BlockSpec((gup.shape[0] // steps, owned), lambda i: (i, 0)),
        pl.BlockSpec((d_rows // steps, gdown.shape[1]), lambda i: (i, 0)),
    ]
    sampler_up, sampler_down = pl.pallas_call(
        copy_kernel,
        grid=(steps,),
        out_shape=(jax.ShapeDtypeStruct(gup.shape, bf16), jax.ShapeDtypeStruct(gdown.shape, bf16)),
        in_specs=blocks,
        out_specs=tuple(blocks),
    )(gup, gdown)

    share = tokens // n_fs
    layer_out = pl.pallas_call(
        functools.partial(sum_kernel, n_fs),
        out_shape=jax.ShapeDtypeStruct((share, width), bf16),
        in_specs=[vmem, vmem],
        out_specs=vmem,
        scratch_shapes=[pltpu.VMEM((n_fs, share, width), bf16), dma((n_fs - 1,)), dma((n_fs,))],
        compiler_params=pltpu.CompilerParams(collective_id=1, has_side_effects=True),
    )(parts.reshape(n_fs, share, width), post_gain[None])
    return (layer_out[None], sampler_up, sampler_down)


def solution(mesh):
    placed = (P("tp", None, None), P("fs", "tp"), P("fs", "tp"), P("fs"), P())
    return jax.shard_map(
        functools.partial(on_device, mesh.shape["fs"], mesh.shape["tp"]),
        mesh=mesh,
        in_specs=placed,
        out_specs=(P("tp", "fs", None), P(None, "fs"), P("fs", None)),
        check_vma=False,
    )
```

profile of v0, /device:TPU:13, one launch (start us, length us, event | category | flops | bytes accessed | tf_op | source)
XLA Modules:
  0.0 277.3 jit_solution(11021396355126294380)
XLA Ops:
  0.6 0.0 copy-start
  0.6 6.8 %multiply_convert_fusion.up = bf16[512,4096]{1,0:T(8,128)(2,1)} fusion(f32[512,4096]{1,0:T(8,128)} %param.6, f32[512]{0:T(512)} %param.8), kind=kLoop, calls=%fused_computation | loop fusion | flops 4194304 | bytes 12584960 | tf_op jit(solution)/shard_map/convert_element_type | solution.py:252
  7.5 0.0 copy-done
  7.5 2.7 convert_element_type.7.down
  10.1 202.8 %shard_map.76 = (bf16[4096,2048]{1,0:T(8,128)(2,1)}, bf16[2048,4096]{1,0:T(8,128)(2,1)}, bf16[128,4096]{1,0:T(8,128)(2,1)}) custom-call(bf16[512,4096]{1,0:T(8,128)(2,1)} %multiply_convert_fusion.up, bf16[2048,1024]{1,0:T(8,128)(2,1)} %convert_element_type.7.down, bf16[128,4096]{1,0:T(8,128)(2,1)} %bitcast.4), custom_call_target="tpu_custom_call" | custom-call | tf_op jit(solution)/shard_map/pallas_call | solution.py:264
  212.9 41.2 %shard_map.77 = bf16[16,4096]{1,0:T(8,128)(2,1)} custom-call(bf16[8,16,4096]{2,1,0:T(8,128)(2,1)} %bitcast.5, f32[1,4096]{1,0:T(1,128)} %bitcast.7), custom_call_target="tpu_custom_call" | custom-call | tf_op jit(solution)/shard_map/pallas_call | solution.py:304
  254.1 0.0 copy-start.1
  254.1 22.6 %shard_map.78 = (bf16[4096,2048]{1,0:T(8,128)(2,1)}, bf16[2048,4096]{1,0:T(8,128)(2,1)}) custom-call(bf16[4096,2048]{1,0:T(8,128)(2,1)} %get-tuple-element.9.up, bf16[2048,4096]{1,0:T(8,128)(2,1)} %get-tuple-element.10.down), custom_call_target="tpu_custom_call" | custom-call | tf_op jit(solution)/shard_map/pallas_call | solution.py:295
  276.7 0.0 copy-done.1
  276.7 0.7 copy.9
Async XLA Ops:
  0.6 6.8 %copy-start = (f32[2048,1024]{1,0:T(8,128)S(1)}, f32[2048,1024]{1,0:T(8,128)}, u32[]{:S(2)}) copy-start(f32[2048,1024]{1,0:T(8,128)} %param.7) | copy-start | bytes 25165828
  254.1 22.6 %copy-start.1 = (bf16[16,4096]{1,0:T(8,128)(2,1)S(1)}, bf16[16,4096]{1,0:T(8,128)(2,1)}, u32[]{:S(2)}) copy-start(bf16[16,4096]{1,0:T(8,128)(2,1)} %shard_map.77) | copy-start | bytes 393220
where the time goes:
time: 278 us; the launch traced here: 277 us
  Pallas kernels  267 us (96%)
  other arithmetic  9.49 us (3%)
    pallas_call x1, Pallas kernels, on_device(): pl.pallas_call(functools.partial(spread_kernel, n_fs, n_tp, n_r), out_sha...  203 us
    pallas_call x1, Pallas kernels, on_device(): pl.pallas_call(functools.partial(sum_kernel, n_fs), out_shape=jax.ShapeDt...  41.2 us
    pallas_call x1, Pallas kernels, on_device(): pl.pallas_call(copy_kernel, grid=(steps,), out_shape=(jax.ShapeDtypeStruc...  22.6 us
    convert_element_type x1, other arithmetic, on_device(): up = (pre_gain[:, None] * trained_up).astype(bf16)  6.81 us

commit v1 on v0

v1 whole, which is shorter than its diff:
```python
import functools

import jax
import jax.numpy as jnp
from jax import lax
from jax.experimental import pallas as pl
from jax.experimental.pallas import tpu as pltpu
from jax.sharding import PartitionSpec as P

MESH = pl.DeviceIdType.MESH
EPS = 1e-06
CHUNK = 256
SEGMENTS = 4
GROUP = 4


def remote(src, dst, send_sem, recv_sem, device):
    return pltpu.make_async_remote_copy(
        src_ref=src, dst_ref=dst, send_sem=send_sem, recv_sem=recv_sem, device_id=device, device_id_type=MESH
    )


def greet(device):
    pl.semaphore_signal(pltpu.get_barrier_semaphore(), inc=1, device_id=device, device_id_type=MESH)


def loop(count, body):
    lax.fori_loop(0, count, lambda i, c: (body(i), c)[1], 0)


def span(i, size):
    return pl.ds(pl.multiple_of(i * size, size), size)


def square_norm(values):
    return values * lax.rsqrt(jnp.mean(values * values, axis=-1, keepdims=True) + EPS)


def spread_kernel(
    n_fs, n_tp, w, fused,
    up_in, down_in, tokens, gain, post, held_up, held_down, out,
    stage, dstage, upb, xup, gcol, normed, acc, hid, pacc, us, ds_in,
    xs, xr, ps, pr, ws, wr, ns, nr, ds, dr, vs, vr, *reduce_refs,
):
    f, t = lax.axis_index("fs"), lax.axis_index("tp")
    far = lax.rem(t + n_tp // 2, n_tp)
    near = t + 1 - 2 * lax.rem(t, 2)
    near_far = lax.rem(near + n_tp // 2, n_tp)
    m = n_fs // n_tp
    rows, cols = up_in.shape
    owned = cols // m
    d_rows, d_width = down_in.shape
    width = n_tp * d_width
    n_c = owned // w
    d_part = d_rows // n_c
    pieces = m * n_c
    block_of_f = f // m
    active = lax.rem(lax.rem(block_of_f, 2) + lax.rem(t, 2), 2) == 0

    def load_up(k):
        return pltpu.make_async_copy(
            up_in.at[:, span(lax.rem(k, m) * n_c + k // m, w)], stage.at[k], us.at[k]
        )

    def load_down(c):
        return pltpu.make_async_copy(down_in.at[span(c, d_part)], dstage.at[lax.rem(c, 2)], ds_in.at[lax.rem(c, 2)])

    def landed(source, c):
        return held_up.at[span(source, rows), span(c, w)]

    def x_copy(k):
        return remote(upb.at[k], xup.at[k], xs.at[k], xr.at[k], {"tp": far})

    def owner(phase, k):
        return (t if phase == 0 else far) * m + lax.rem(k, m)

    def peer_copy(phase, k):
        held = upb if phase == 0 else xup
        return remote(held.at[k], landed(f, k // m), ps.at[phase, k], pr.at[f, k // m], {"fs": owner(phase, k)})

    def start_peer(phase, k):
        @pl.when(owner(phase, k) != f)
        def _():
            peer_copy(phase, k).start()

    def end_peer(phase, k):
        @pl.when(owner(phase, k) != f)
        def _():
            peer_copy(phase, k).wait_send()

    def block(c, which):
        return held_down.at[span(c, d_part), span(which, d_width)]

    def d_copy(c):
        return remote(block(c, t), block(c, t), ds.at[c], dr.at[c], {"tp": far})

    def d_pass(c, which):
        return remote(block(c, which), block(c, which), vs.at[c], vr.at[c], {"tp": near})

    def column(which):
        return held_down.at[:, span(which, d_width)]

    def to_near(which):
        return remote(column(which), column(which), ns, nr, {"tp": near})

    def share(src, source, c):
        return remote(src, landed(source, c), ws.at[source, c], wr.at[source, c], {"tp": near})

    loop(n_fs - 1, lambda i: greet({"fs": lax.rem(f + 1 + i, n_fs)}))
    greet({"tp": far})
    greet({"tp": near})
    loop(pieces, lambda k: load_up(k).start())
    for c in range(min(2, n_c)):
        load_down(c).start()

    side = min(rows, 128)
    eye = lax.broadcasted_iota(jnp.int32, (side, side), 0) == lax.broadcasted_iota(jnp.int32, (side, side), 1)
    for b in range(rows // side):
        line = jnp.broadcast_to(gain[:, b * side : (b + 1) * side], (side, side))
        scale = jnp.sum(jnp.where(eye, line, 0.0), axis=1, keepdims=True)
        gcol[b * side : (b + 1) * side, :] = jnp.broadcast_to(scale, (side, 128))

    def convert(k):
        load_up(k).wait()
        for j in range(0, w, 128):
            upb[k, :, j : j + 128] = (gcol[...] * stage[k, :, j : j + 128]).astype(upb.dtype)

    def send(k):
        x_copy(k).start()
        start_peer(0, k)

    convert(0)
    pl.semaphore_wait(pltpu.get_barrier_semaphore(), n_fs + 1)

    def convert_and_send(k):
        convert(k)
        send(k - 1)

    lax.fori_loop(1, pieces, lambda k, c: (convert_and_send(k), c)[1], 0)
    pacc[...] = jnp.zeros_like(pacc)
    send(pieces - 1)

    def convert_down(c):
        load_down(c).wait()
        held_down[span(c, d_part), span(t, d_width)] = dstage[lax.rem(c, 2)].astype(held_down.dtype)

        @pl.when(c + 2 < n_c)
        def _():
            load_down(c + 2).start()

    def pass_on(k):
        @pl.when(k == max(pieces - 2, 0))
        def _():
            loop(n_c, lambda c: d_copy(c).start())
            to_near(t).start()

        x_copy(k).wait_recv()
        start_peer(1, k)

        @pl.when(k < n_c)
        def _():
            convert_down(k)

        @pl.when(k == n_c)
        def _():
            scaled = square_norm(tokens[...].astype(jnp.float32)).astype(jnp.bfloat16)
            for i in range(n_fs):
                normed[i] = scaled[:, i * rows : (i + 1) * rows]

    loop(pieces, pass_on)

    def gather(c):
        remote(block(c, far), block(c, far), ds.at[c], dr.at[c], {"tp": far}).wait_recv()
        d_pass(c, far).start()
        acc[...] = jnp.zeros_like(acc)

        def one(source):
            def keep_own(held):
                k = c * m + lax.rem(f, m)
                share(held.at[k], source, c).start()
                held_up[span(source, rows), span(c, w)] = held[k]

            @pl.when(jnp.logical_and(active, source == f))
            def _():
                @pl.when(block_of_f == t)
                def _():
                    keep_own(upb)

                @pl.when(block_of_f != t)
                def _():
                    keep_own(xup)

            @pl.when(jnp.logical_and(active, source != f))
            def _():
                remote(landed(source, c), landed(source, c), ws.at[source, c], pr.at[source, c], {"tp": near}).wait_recv()
                share(landed(source, c), source, c).start()

            @pl.when(jnp.logical_not(active))
            def _():
                share(landed(source, c), source, c).wait_recv()

            acc[...] += jnp.dot(
                normed[source], held_up[span(source, rows), span(c, w)], preferred_element_type=jnp.float32
            )

        loop(n_fs, one)
        hid[...] = jnp.square(jnp.maximum(acc[...], 0.0)).astype(jnp.bfloat16)
        d_pass(c, near_far).wait_recv()

        @pl.when(c == 0)
        def _():
            to_near(near).wait_recv()

    def add_down(c, first, count):
        tile = min(d_width, 512)

        def one(i):
            at = pl.ds(pl.multiple_of(first + i * tile, tile), tile)
            pacc[:, at] += jnp.dot(hid[...], held_down[span(c, d_part), at], preferred_element_type=jnp.float32)

        loop(count // tile, one)

    def whole_chunk(c):
        gather(c)
        add_down(c, 0, width)

    last = n_c - 1
    loop(last, whole_chunk)
    gather(last)
    if fused:
        sb, land, sb2, land2, fin, ss, rs, ss2, rs2 = reduce_refs
        _, q, n_o, part, seg = sb.shape
        i, o = lax.rem(f, q), f // q

        def peer(d):
            return lax.rem(i + d, q)

        def across(d):
            return lax.rem(o + d, n_o)

        def first_copy(s, d):
            return remote(sb.at[s, peer(d)], land.at[s, i], ss.at[s, d], rs.at[s, i], {"fs": o * q + peer(d)})

        def second_copy(s, d):
            return remote(sb2.at[s, across(d)], land2.at[s, o], ss2.at[s, d], rs2.at[s, o], {"fs": across(d) * q + i})

        for s in range(SEGMENTS):
            add_down(last, s * seg, seg)
            for b in range(n_o * q):
                sb[s, b % q, b // q] = pacc[b * part : (b + 1) * part, s * seg : (s + 1) * seg].astype(sb.dtype)
            for d in range(1, q):
                first_copy(s, d).start()

        for s in range(SEGMENTS):
            for d in range(1, q):
                remote(land.at[s, peer(d)], land.at[s, peer(d)], ss.at[s, d], rs.at[s, peer(d)], {"fs": f}).wait_recv()

            def total(to):
                value = pacc[span(to * q + i, part), s * seg : (s + 1) * seg]
                for d in range(1, q):
                    value += land[s, peer(d), to].astype(jnp.float32)
                return value

            for d in range(1, n_o):
                sb2[s, across(d)] = total(across(d)).astype(sb2.dtype)
            fin[:, s * seg : (s + 1) * seg] = total(o)
            for d in range(1, n_o):
                second_copy(s, d).start()

        for s in range(SEGMENTS):
            value = fin[:, s * seg : (s + 1) * seg]
            for d in range(1, n_o):
                remote(land2.at[s, across(d)], land2.at[s, across(d)], ss2.at[s, d], rs2.at[s, across(d)], {"fs": f}).wait_recv()
                value += land2[s, across(d)].astype(jnp.float32)
            fin[:, s * seg : (s + 1) * seg] = value
        total_sum = fin[...]
        scale = lax.rsqrt(jnp.mean(total_sum * total_sum, axis=-1, keepdims=True) + EPS)
        out[...] = (total_sum * scale * post[...]).astype(out.dtype)
        for s in range(SEGMENTS):
            for d in range(1, q):
                first_copy(s, d).wait_send()
            for d in range(1, n_o):
                second_copy(s, d).wait_send()
    else:
        add_down(last, 0, width)
        out[...] = pacc[...].astype(out.dtype)

    def ended(i):
        @pl.when(active)
        def _():
            source, c = i // n_c, lax.rem(i, n_c)
            share(landed(source, c), source, c).wait_send()

    loop(n_fs * n_c, ended)
    to_near(t).wait_send()

    def ended_down(c):
        d_copy(c).wait_send()
        d_pass(c, far).wait_send()

    loop(n_c, ended_down)

    def ended_pieces(k):
        x_copy(k).wait_send()
        end_peer(0, k)
        end_peer(1, k)

    loop(pieces, ended_pieces)


def sum_kernel(n_fs, parts, gain, out, land, ss, rs):
    f = lax.axis_index("fs")

    def peer_of(i):
        return lax.rem(f + 1 + i, n_fs)

    loop(n_fs - 1, lambda i: greet({"fs": peer_of(i)}))
    pl.semaphore_wait(pltpu.get_barrier_semaphore(), n_fs - 1)

    def send(i):
        return remote(parts.at[peer_of(i)], land.at[f], ss.at[i], rs.at[f], {"fs": peer_of(i)})

    loop(n_fs - 1, lambda i: send(i).start())

    def add(i, total):
        source = peer_of(i)
        remote(land.at[source], land.at[source], ss.at[i], rs.at[source], {"fs": source}).wait_recv()
        return total + land[source].astype(jnp.float32)

    summed = lax.fori_loop(0, n_fs - 1, add, parts[f].astype(jnp.float32))
    scale = lax.rsqrt(jnp.mean(summed * summed, axis=-1, keepdims=True) + EPS)
    out[...] = (summed * scale * gain[...]).astype(out.dtype)
    loop(n_fs - 1, lambda i: send(i).wait_send())


def on_device(n_fs, n_tp, prompt_tokens, trained_up, trained_down, pre_gain, post_gain):
    bf16, f32 = jnp.bfloat16, jnp.float32
    rows, cols = trained_up.shape
    d_rows, d_cols = trained_down.shape
    tokens, width = prompt_tokens.shape[1:]
    m = n_fs // n_tp
    owned = cols // m
    w = min(owned, CHUNK)
    n_c = owned // w
    pieces = m * n_c
    share = tokens // n_fs
    q = GROUP
    n_o = n_fs // q
    seg = width // SEGMENTS
    fused = share % 16 == 0 and n_fs % q == 0 and n_o > 1
    anywhere = pl.BlockSpec(memory_space=pl.ANY)
    vmem = pl.BlockSpec(memory_space=pltpu.VMEM)
    dma = pltpu.SemaphoreType.DMA
    reduce_scratch = [
        pltpu.VMEM((SEGMENTS, q, n_o, share, seg), bf16),
        pltpu.VMEM((SEGMENTS, q, n_o, share, seg), bf16),
        pltpu.VMEM((SEGMENTS, n_o, share, seg), bf16),
        pltpu.VMEM((SEGMENTS, n_o, share, seg), bf16),
        pltpu.VMEM((share, width), f32),
        dma((SEGMENTS, q)), dma((SEGMENTS, q)),
        dma((SEGMENTS, n_o)), dma((SEGMENTS, n_o)),
    ]
    sampler_up, sampler_down, result = pl.pallas_call(
        functools.partial(spread_kernel, n_fs, n_tp, w, fused),
        out_shape=(
            pltpu.VMEM((n_fs * rows, owned), bf16),
            pltpu.VMEM((d_rows, n_tp * d_cols), bf16),
            jax.ShapeDtypeStruct((share if fused else tokens, width), bf16),
        ),
        in_specs=[anywhere, anywhere, vmem, vmem, vmem],
        out_specs=(vmem, vmem, vmem),
        scratch_shapes=[
            pltpu.VMEM((pieces, rows, w), f32),
            pltpu.VMEM((2, d_rows // n_c, d_cols), f32),
            pltpu.VMEM((pieces, rows, w), bf16),
            pltpu.VMEM((pieces, rows, w), bf16),
            pltpu.VMEM((rows, 128), f32),
            pltpu.VMEM((n_fs, tokens, rows), bf16),
            pltpu.VMEM((tokens, w), f32),
            pltpu.VMEM((tokens, w), bf16),
            pltpu.VMEM((tokens, width), f32),
            dma((pieces,)), dma((2,)),
            dma((pieces,)), dma((pieces,)),
            dma((2, pieces)), dma((n_fs, n_c)),
            dma((n_fs, n_c)), dma((n_fs, n_c)),
            dma, dma,
            dma((n_c,)), dma((n_c,)),
            dma((n_c,)), dma((n_c,)),
        ] + (reduce_scratch if fused else []),
        compiler_params=pltpu.CompilerParams(collective_id=0, has_side_effects=True, vmem_limit_bytes=32000000),
    )(trained_up, trained_down, prompt_tokens[0], pre_gain[None], post_gain[None])
    if fused:
        return (result[None], sampler_up, sampler_down)

    layer_out = pl.pallas_call(
        functools.partial(sum_kernel, n_fs),
        out_shape=jax.ShapeDtypeStruct((share, width), bf16),
        in_specs=[vmem, vmem],
        out_specs=vmem,
        scratch_shapes=[pltpu.VMEM((n_fs, share, width), bf16), dma((n_fs - 1,)), dma((n_fs,))],
        compiler_params=pltpu.CompilerParams(collective_id=1, has_side_effects=True, vmem_limit_bytes=16000000),
    )(result.reshape(n_fs, share, width), post_gain[None])
    return (layer_out[None], sampler_up, sampler_down)


def solution(mesh):
    placed = (P("tp", None, None), P("fs", "tp"), P("fs", "tp"), P("fs"), P())
    return jax.shard_map(
        functools.partial(on_device, mesh.shape["fs"], mesh.shape["tp"]),
        mesh=mesh,
        in_specs=placed,
        out_specs=(P("tp", "fs", None), P(None, "fs"), P("fs", None)),
        check_vma=False,
    )
```

time: 278 us -> 234 us (0.84)
  Pallas kernels: 267 us -> 220 us
  local copies, waits for them, and re-layouts: 0.66 us -> 13 us
  other arithmetic: 9.49 us -> 0 us
    pallas_call x3 -> x1, Pallas kernels: 267 us -> 220 us  [on_device(): pl.pallas_call(functools.partial(spread_kernel, n_fs, n_tp, w, fused), ou...]
    unnamed x5, local copies, waits for them, and re-layouts: 0.66 us -> 13 us
    convert_element_type x2 -> x0, other arithmetic: 9.49 us -> none  [the longest x1 6.81 us: on_device(): up = (pre_gain[:, None] * trained_up).astype(bf16)]
where the time goes in v1:
time: 234 us
  Pallas kernels  220 us (94%)
  local copies, waits for them, and re-layouts  13 us (6%)
    pallas_call x1, Pallas kernels, on_device(): pl.pallas_call(functools.partial(spread_kernel, n_fs, n_tp, w, fused), ou...  220 us
    unnamed x5, local copies, waits for them, and re-layouts  13 us

profile of v1, /device:TPU:13, one launch (start us, length us, event | category | flops | bytes accessed | tf_op | source)
XLA Modules:
  0.0 234.0 jit_solution(5683861049434212853)
XLA Ops:
  0.6 220.3 %shard_map.76 = (bf16[4096,2048]{1,0:T(8,128)(2,1)S(1)}, bf16[2048,4096]{1,0:T(8,128)(2,1)S(1)}, bf16[16,4096]{1,0:T(8,128)(2,1)}) custom-call(f32[512,4096]{1,0:T(8,128)} %up_in.1, f32[2048,1024]{1,0:T(8,128)} %down_in.1, bf16[128,4096]{1,0:T(8,128)(2,1)} %bitcast.4, f32[1,512]{1,0:T(1,128)} %bitcast.7, f32[1,4096]{1,0:T(1,128)} %bitcast.6), custom_call_target="tpu_custom_call" | custom-call | tf_op jit(solution)/shard_map/pallas_call | solution.py:363
  221.0 6.2 %copy.11 = bf16[4096,2048]{1,0:T(8,128)(2,1)} copy(bf16[4096,2048]{1,0:T(8,128)(2,1)S(1)} %get-tuple-element.10) | data formatting | bytes 33554432
  227.1 0.0 copy-start
  227.2 6.2 %copy.12 = bf16[2048,4096]{1,0:T(8,128)(2,1)} copy(bf16[2048,4096]{1,0:T(8,128)(2,1)S(1)} %get-tuple-element.11) | data formatting | bytes 33554432
  233.3 0.0 copy-done
  233.3 0.7 copy.13
Async XLA Ops:
  227.1 6.2 %copy-start = (bf16[16,4096]{1,0:T(8,128)(2,1)S(1)}, bf16[16,4096]{1,0:T(8,128)(2,1)}, u32[]{:S(2)}) copy-start(bf16[16,4096]{1,0:T(8,128)(2,1)} %get-tuple-element.6) | copy-start | bytes 393220

commit v2 on v1

--- a/solution.py
+++ b/solution.py
@@ -12,6 +12,8 @@
 CHUNK = 256
 SEGMENTS = 4
 GROUP = 4
+PARTS = 4
+DEPTH = 4
 
 
 def remote(src, dst, send_sem, recv_sem, device):
@@ -68,25 +70,32 @@
     def landed(source, c):
         return held_up.at[span(source, rows), span(c, w)]
 
-    def x_copy(k):
-        return remote(upb.at[k], xup.at[k], xs.at[k], xr.at[k], {"tp": far})
+    n_s = PARTS if rows % (16 * PARTS) == 0 else 1
+    sub = rows // n_s
+
+    def x_copy(k, r):
+        at = pl.ds(r * sub, sub)
+        return remote(upb.at[k, at], xup.at[k, at], xs.at[k], xr.at[k, r], {"tp": far})
 
     def owner(phase, k):
         return (t if phase == 0 else far) * m + lax.rem(k, m)
 
-    def peer_copy(phase, k):
+    def peer_copy(phase, k, first, size):
         held = upb if phase == 0 else xup
-        return remote(held.at[k], landed(f, k // m), ps.at[phase, k], pr.at[f, k // m], {"fs": owner(phase, k)})
-
-    def start_peer(phase, k):
+        to = held_up.at[pl.ds(pl.multiple_of(f * rows + first, size), size), span(k // m, w)]
+        return remote(
+            held.at[k, pl.ds(first, size)], to, ps.at[phase, k], pr.at[f, k // m], {"fs": owner(phase, k)}
+        )
+
+    def start_peer(phase, k, r):
         @pl.when(owner(phase, k) != f)
         def _():
-            peer_copy(phase, k).start()
+            peer_copy(phase, k, r * sub, sub).start()
 
     def end_peer(phase, k):
         @pl.when(owner(phase, k) != f)
         def _():
-            peer_copy(phase, k).wait_send()
+            peer_copy(phase, k, 0, rows).wait_send()
 
     def block(c, which):
         return held_down.at[span(c, d_part), span(which, d_width)]
@@ -109,7 +118,8 @@
     loop(n_fs - 1, lambda i: greet({"fs": lax.rem(f + 1 + i, n_fs)}))
     greet({"tp": far})
     greet({"tp": near})
-    loop(pieces, lambda k: load_up(k).start())
+    depth = min(DEPTH, pieces)
+    loop(depth, lambda k: load_up(k).start())
     for c in range(min(2, n_c)):
         load_down(c).start()
 
@@ -122,12 +132,19 @@
 
     def convert(k):
         load_up(k).wait()
+
+        @pl.when(k + depth < pieces)
+        def _():
+            load_up(k + depth).start()
+
         for j in range(0, w, 128):
             upb[k, :, j : j + 128] = (gcol[...] * stage[k, :, j : j + 128]).astype(upb.dtype)
 
     def send(k):
-        x_copy(k).start()
-        start_peer(0, k)
+        for r in range(n_s):
+            x_copy(k, r).start()
+        for r in range(n_s):
+            start_peer(0, k, r)
 
     convert(0)
     pl.semaphore_wait(pltpu.get_barrier_semaphore(), n_fs + 1)
@@ -154,8 +171,9 @@
             loop(n_c, lambda c: d_copy(c).start())
             to_near(t).start()
 
-        x_copy(k).wait_recv()
-        start_peer(1, k)
+        for r in range(n_s):
+            x_copy(k, r).wait_recv()
+            start_peer(1, k, r)
 
         @pl.when(k < n_c)
         def _():
@@ -301,7 +319,7 @@
     loop(n_c, ended_down)
 
     def ended_pieces(k):
-        x_copy(k).wait_send()
+        remote(upb.at[k], xup.at[k], xs.at[k], xr.at[k, 0], {"tp": far}).wait_send()
         end_peer(0, k)
         end_peer(1, k)
 
@@ -380,7 +398,7 @@
             pltpu.VMEM((tokens, w), bf16),
             pltpu.VMEM((tokens, width), f32),
             dma((pieces,)), dma((2,)),
-            dma((pieces,)), dma((pieces,)),
+            dma((pieces,)), dma((pieces, PARTS)),
             dma((2, pieces)), dma((n_fs, n_c)),
             dma((n_fs, n_c)), dma((n_fs, n_c)),
             dma, dma,

time: 234 us -> 231 us (0.987)
  Pallas kernels: 220 us -> 217 us
    pallas_call x1, Pallas kernels: 220 us -> 217 us  [on_device(): pl.pallas_call(functools.partial(spread_kernel, n_fs, n_tp, w, fused), ou...]
where the time goes in v2:
time: 231 us; the launch traced here: 230 us
  Pallas kernels  217 us (94%)
  local copies, waits for them, and re-layouts  13 us (6%)
    pallas_call x1, Pallas kernels, on_device(): pl.pallas_call(functools.partial(spread_kernel, n_fs, n_tp, w, fused), ou...  217 us
    unnamed x5, local copies, waits for them, and re-layouts  13 us

profile of v2, /device:TPU:13, one launch (start us, length us, event | category | flops | bytes accessed | tf_op | source)
XLA Modules:
  0.0 230.2 jit_solution(13581985968892028559)
XLA Ops:
  0.6 216.6 %shard_map.76 = (bf16[4096,2048]{1,0:T(8,128)(2,1)S(1)}, bf16[2048,4096]{1,0:T(8,128)(2,1)S(1)}, bf16[16,4096]{1,0:T(8,128)(2,1)}) custom-call(f32[512,4096]{1,0:T(8,128)} %up_in.1, f32[2048,1024]{1,0:T(8,128)} %down_in.1, bf16[128,4096]{1,0:T(8,128)(2,1)} %bitcast.4, f32[1,512]{1,0:T(1,128)} %bitcast.7, f32[1,4096]{1,0:T(1,128)} %bitcast.6), custom_call_target="tpu_custom_call" | custom-call | tf_op jit(solution)/shard_map/pallas_call | solution.py:381
  217.2 6.2 %copy.11 = bf16[4096,2048]{1,0:T(8,128)(2,1)} copy(bf16[4096,2048]{1,0:T(8,128)(2,1)S(1)} %get-tuple-element.10) | data formatting | bytes 33554432
  223.4 0.0 copy-start
  223.4 6.2 %copy.12 = bf16[2048,4096]{1,0:T(8,128)(2,1)} copy(bf16[2048,4096]{1,0:T(8,128)(2,1)S(1)} %get-tuple-element.11) | data formatting | bytes 33554432
  229.5 0.0 copy-done
  229.5 0.7 copy.13
Async XLA Ops:
  223.4 6.2 %copy-start = (bf16[16,4096]{1,0:T(8,128)(2,1)S(1)}, bf16[16,4096]{1,0:T(8,128)(2,1)}, u32[]{:S(2)}) copy-start(bf16[16,4096]{1,0:T(8,128)(2,1)} %get-tuple-element.6) | copy-start | bytes 393220

commit v3 on v2

--- a/solution.py
+++ b/solution.py
@@ -12,6 +12,7 @@
 CHUNK = 256
 SEGMENTS = 4
 GROUP = 4
+STORES = 4
 PARTS = 4
 DEPTH = 4
 
@@ -40,8 +41,8 @@
 
 def spread_kernel(
     n_fs, n_tp, w, fused,
-    up_in, down_in, tokens, gain, post, held_up, held_down, out,
-    stage, dstage, upb, xup, gcol, normed, acc, hid, pacc, us, ds_in,
+    up_in, down_in, tokens, gain, post, held_up, held_down, pacc, out,
+    stage, dstage, upb, xup, gcol, normed, acc, hid, us, ds_in,
     xs, xr, ps, pr, ws, wr, ns, nr, ds, dr, vs, vr, *reduce_refs,
 ):
     f, t = lax.axis_index("fs"), lax.axis_index("tp")
@@ -192,7 +193,11 @@
         d_pass(c, far).start()
         acc[...] = jnp.zeros_like(acc)
 
-        def one(source):
+        def one(step):
+            half = n_fs // 2
+            side = lax.rem(f // half + step // half, 2)
+            source = side * half + lax.rem(f + step, half)
+
             def keep_own(held):
                 k = c * m + lax.rem(f, m)
                 share(held.at[k], source, c).start()
@@ -246,62 +251,16 @@
     loop(last, whole_chunk)
     gather(last)
     if fused:
-        sb, land, sb2, land2, fin, ss, rs, ss2, rs2 = reduce_refs
-        _, q, n_o, part, seg = sb.shape
-        i, o = lax.rem(f, q), f // q
-
-        def peer(d):
-            return lax.rem(i + d, q)
-
-        def across(d):
-            return lax.rem(o + d, n_o)
-
-        def first_copy(s, d):
-            return remote(sb.at[s, peer(d)], land.at[s, i], ss.at[s, d], rs.at[s, i], {"fs": o * q + peer(d)})
-
-        def second_copy(s, d):
-            return remote(sb2.at[s, across(d)], land2.at[s, o], ss2.at[s, d], rs2.at[s, o], {"fs": across(d) * q + i})
-
-        for s in range(SEGMENTS):
-            add_down(last, s * seg, seg)
-            for b in range(n_o * q):
-                sb[s, b % q, b // q] = pacc[b * part : (b + 1) * part, s * seg : (s + 1) * seg].astype(sb.dtype)
-            for d in range(1, q):
-                first_copy(s, d).start()
-
-        for s in range(SEGMENTS):
-            for d in range(1, q):
-                remote(land.at[s, peer(d)], land.at[s, peer(d)], ss.at[s, d], rs.at[s, peer(d)], {"fs": f}).wait_recv()
-
-            def total(to):
-                value = pacc[span(to * q + i, part), s * seg : (s + 1) * seg]
-                for d in range(1, q):
-                    value += land[s, peer(d), to].astype(jnp.float32)
-                return value
-
-            for d in range(1, n_o):
-                sb2[s, across(d)] = total(across(d)).astype(sb2.dtype)
-            fin[:, s * seg : (s + 1) * seg] = total(o)
-            for d in range(1, n_o):
-                second_copy(s, d).start()
-
-        for s in range(SEGMENTS):
-            value = fin[:, s * seg : (s + 1) * seg]
-            for d in range(1, n_o):
-                remote(land2.at[s, across(d)], land2.at[s, across(d)], ss2.at[s, d], rs2.at[s, across(d)], {"fs": f}).wait_recv()
-                value += land2[s, across(d)].astype(jnp.float32)
-            fin[:, s * seg : (s + 1) * seg] = value
-        total_sum = fin[...]
-        scale = lax.rsqrt(jnp.mean(total_sum * total_sum, axis=-1, keepdims=True) + EPS)
-        out[...] = (total_sum * scale * post[...]).astype(out.dtype)
-        for s in range(SEGMENTS):
-            for d in range(1, q):
-                first_copy(s, d).wait_send()
-            for d in range(1, n_o):
-                second_copy(s, d).wait_send()
+        @pl.when(lax.rem(t, 2) == 0)
+        def _():
+            reduce_rows(pacc, post, out, lambda s, seg: add_down(last, s * seg, seg), *reduce_refs)
+
+        @pl.when(lax.rem(t, 2) == 1)
+        def _():
+            add_down(last, 0, width)
     else:
         add_down(last, 0, width)
-        out[...] = pacc[...].astype(out.dtype)
+        out[...] = jnp.zeros_like(out)
 
     def ended(i):
         @pl.when(active)
@@ -324,6 +283,113 @@
         end_peer(1, k)
 
     loop(pieces, ended_pieces)
+
+
+def reduce_rows(pacc, post, out, compute, sb, land, sb2, land2, fin, ss, rs, ss2, rs2):
+    f = lax.axis_index("fs")
+    _, q, n_o, part, seg = sb.shape
+    i, o = lax.rem(f, q), f // q
+
+    def peer(d):
+        return lax.rem(i + d, q)
+
+    def across(d):
+        return lax.rem(o + d, n_o)
+
+    def first_copy(s, d):
+        return remote(sb.at[s, peer(d)], land.at[s, i], ss.at[s, d], rs.at[s, i], {"fs": o * q + peer(d)})
+
+    def second_copy(s, d):
+        return remote(sb2.at[s, across(d)], land2.at[s, o], ss2.at[s, d], rs2.at[s, o], {"fs": across(d) * q + i})
+
+    def fill(s):
+        for b in range(n_o * q):
+            sb[s, b % q, b // q] = pacc[b * part : (b + 1) * part, s * seg : (s + 1) * seg].astype(sb.dtype)
+
+    def send(s):
+        for d in range(1, q):
+            first_copy(s, d).start()
+
+    if compute is None:
+        for s in range(SEGMENTS):
+            fill(s)
+        pl.semaphore_wait(pltpu.get_barrier_semaphore(), n_o * q - 1)
+        for s in range(SEGMENTS):
+            send(s)
+    else:
+        for s in range(SEGMENTS):
+            compute(s, seg)
+            fill(s)
+            send(s)
+
+    for s in range(SEGMENTS):
+        for d in range(1, q):
+            remote(land.at[s, peer(d)], land.at[s, peer(d)], ss.at[s, d], rs.at[s, peer(d)], {"fs": f}).wait_recv()
+
+        def total(to):
+            value = pacc[span(to * q + i, part), s * seg : (s + 1) * seg]
+            for d in range(1, q):
+                value += land[s, peer(d), to].astype(jnp.float32)
+            return value
+
+        for d in range(1, n_o):
+            sb2[s, across(d)] = total(across(d)).astype(sb2.dtype)
+        fin[:, s * seg : (s + 1) * seg] = total(o)
+        for d in range(1, n_o):
+            second_copy(s, d).start()
+
+    for s in range(SEGMENTS):
+        value = fin[:, s * seg : (s + 1) * seg]
+        for d in range(1, n_o):
+            remote(land2.at[s, across(d)], land2.at[s, across(d)], ss2.at[s, d], rs2.at[s, across(d)], {"fs": f}).wait_recv()
+            value += land2[s, across(d)].astype(jnp.float32)
+        fin[:, s * seg : (s + 1) * seg] = value
+    summed = fin[...]
+    scale = lax.rsqrt(jnp.mean(summed * summed, axis=-1, keepdims=True) + EPS)
+    out[...] = (summed * scale * post[...]).astype(out.dtype)
+    for s in range(SEGMENTS):
+        for d in range(1, q):
+            first_copy(s, d).wait_send()
+        for d in range(1, n_o):
+            second_copy(s, d).wait_send()
+
+
+def late_kernel(n_fs, pacc, post, early, up_token, down_token, out, *refs):
+    f, t = lax.axis_index("fs"), lax.axis_index("tp")
+
+    @pl.when(lax.rem(t, 2) == 1)
+    def _():
+        loop(n_fs - 1, lambda i: greet({"fs": lax.rem(f + 1 + i, n_fs)}))
+        reduce_rows(pacc, post, out, None, *refs)
+
+    @pl.when(lax.rem(t, 2) == 0)
+    def _():
+        out[...] = early[...]
+
+
+def store_kernel(src, dst, token, sems):
+    count = sems.shape[0]
+    size = src.shape[0] // count
+    copies = [
+        pltpu.make_async_copy(src.at[pl.ds(p * size, size)], dst.at[pl.ds(p * size, size)], sems.at[p])
+        for p in range(count)
+    ]
+    for copy in copies:
+        copy.start()
+    token[...] = jnp.zeros_like(token)
+    for copy in copies:
+        copy.wait()
+
+
+def store(array):
+    return pl.pallas_call(
+        store_kernel,
+        out_shape=(jax.ShapeDtypeStruct(array.shape, array.dtype), jax.ShapeDtypeStruct((8, 128), jnp.float32)),
+        in_specs=[pl.BlockSpec(memory_space=pltpu.VMEM)],
+        out_specs=(pl.BlockSpec(memory_space=pl.ANY), pl.BlockSpec(memory_space=pltpu.VMEM)),
+        scratch_shapes=[pltpu.SemaphoreType.DMA((STORES,))],
+        compiler_params=pltpu.CompilerParams(vmem_limit_bytes=1000000),
+    )(array)
 
 
 def sum_kernel(n_fs, parts, gain, out, land, ss, rs):
@@ -378,15 +444,16 @@
         dma((SEGMENTS, q)), dma((SEGMENTS, q)),
         dma((SEGMENTS, n_o)), dma((SEGMENTS, n_o)),
     ]
-    sampler_up, sampler_down, result = pl.pallas_call(
+    held_up, held_down, parts, early = pl.pallas_call(
         functools.partial(spread_kernel, n_fs, n_tp, w, fused),
         out_shape=(
             pltpu.VMEM((n_fs * rows, owned), bf16),
             pltpu.VMEM((d_rows, n_tp * d_cols), bf16),
-            jax.ShapeDtypeStruct((share if fused else tokens, width), bf16),
+            pltpu.VMEM((tokens, width), f32),
+            jax.ShapeDtypeStruct((share, width), bf16),
         ),
         in_specs=[anywhere, anywhere, vmem, vmem, vmem],
-        out_specs=(vmem, vmem, vmem),
+        out_specs=(vmem, vmem, vmem, vmem),
         scratch_shapes=[
             pltpu.VMEM((pieces, rows, w), f32),
             pltpu.VMEM((2, d_rows // n_c, d_cols), f32),
@@ -396,7 +463,6 @@
             pltpu.VMEM((n_fs, tokens, rows), bf16),
             pltpu.VMEM((tokens, w), f32),
             pltpu.VMEM((tokens, w), bf16),
-            pltpu.VMEM((tokens, width), f32),
             dma((pieces,)), dma((2,)),
             dma((pieces,)), dma((pieces, PARTS)),
             dma((2, pieces)), dma((n_fs, n_c)),
@@ -405,10 +471,20 @@
             dma((n_c,)), dma((n_c,)),
             dma((n_c,)), dma((n_c,)),
         ] + (reduce_scratch if fused else []),
-        compiler_params=pltpu.CompilerParams(collective_id=0, has_side_effects=True, vmem_limit_bytes=32000000),
+        compiler_params=pltpu.CompilerParams(collective_id=0, has_side_effects=True, vmem_limit_bytes=30500000),
     )(trained_up, trained_down, prompt_tokens[0], pre_gain[None], post_gain[None])
+    sampler_up, up_token = store(held_up)
+    sampler_down, down_token = store(held_down)
     if fused:
-        return (result[None], sampler_up, sampler_down)
+        layer_out = pl.pallas_call(
+            functools.partial(late_kernel, n_fs),
+            out_shape=jax.ShapeDtypeStruct((share, width), bf16),
+            in_specs=[vmem, vmem, vmem, anywhere, anywhere],
+            out_specs=vmem,
+            scratch_shapes=reduce_scratch,
+            compiler_params=pltpu.CompilerParams(collective_id=1, has_side_effects=True, vmem_limit_bytes=16000000),
+        )(parts, post_gain[None], early, up_token, down_token)
+        return (layer_out[None], sampler_up, sampler_down)
 
     layer_out = pl.pallas_call(
         functools.partial(sum_kernel, n_fs),
@@ -417,7 +493,7 @@
         out_specs=vmem,
         scratch_shapes=[pltpu.VMEM((n_fs, share, width), bf16), dma((n_fs - 1,)), dma((n_fs,))],
         compiler_params=pltpu.CompilerParams(collective_id=1, has_side_effects=True, vmem_limit_bytes=16000000),
-    )(result.reshape(n_fs, share, width), post_gain[None])
+    )(parts.astype(bf16).reshape(n_fs, share, width), post_gain[None])
     return (layer_out[None], sampler_up, sampler_down)
 
 

time: 231 us -> 227 us (0.983)
  local copies, waits for them, and re-layouts: 13 us -> 0.67 us
  Pallas kernels: 217 us -> 224 us
    pallas_call x0 -> x3, Pallas kernels: none -> 29.5 us  [the longest x1 17.6 us: on_device(): pl.pallas_call(functools.partial(late_kernel, n_fs), out_shape=jax.ShapeD...]
    pallas_call x1, Pallas kernels: 217 us -> 195 us  [on_device(): pl.pallas_call(functools.partial(spread_kernel, n_fs, n_tp, w, fused), ou...]
    unnamed x5, local copies, waits for them, and re-layouts: 13 us -> 0.67 us
where the time goes in v3:
time: 227 us; the launch traced here: 225 us
  Pallas kernels  224 us (99%)
    pallas_call x1, Pallas kernels, on_device(): pl.pallas_call(functools.partial(spread_kernel, n_fs, n_tp, w, fused), ou...  195 us
    pallas_call x1, Pallas kernels, on_device(): pl.pallas_call(functools.partial(late_kernel, n_fs), out_shape=jax.ShapeD...  17.6 us
    pallas_call x2, Pallas kernels, store(): pl.pallas_call(store_kernel, out_shape=(jax.ShapeDtypeStruct(array.shape,...  11.9 us

profile of v3, /device:TPU:13, one launch (start us, length us, event | category | flops | bytes accessed | tf_op | source)
XLA Modules:
  0.0 225.4 jit_solution(9948180755920437944)
XLA Ops:
  0.6 194.6 %shard_map.76 = (bf16[4096,2048]{1,0:T(8,128)(2,1)S(1)}, bf16[2048,4096]{1,0:T(8,128)(2,1)S(1)}, f32[128,4096]{1,0:T(8,128)S(1)}, bf16[16,4096]{1,0:T(8,128)(2,1)}) custom-call(f32[512,4096]{1,0:T(8,128)} %up_in.1, f32[2048,1024]{1,0:T(8,128)} %down_in.1, bf16[128,4096]{1,0:T(8,128)(2,1)} %bitcast.7, f32[1,512]{1,0:T(1,128)} %bitcast.8, f32[1,4096]{1,0:T(1,128)} %bitcast.5), custom_call_target="tpu_custom_call" | custom-call | tf_op jit(solution)/shard_map/pallas_call | solution.py:447
  195.2 0.0 copy-start
  195.2 0.0 copy-start.1
  195.3 6.0 %shard_map.77 = (bf16[4096,2048]{1,0:T(8,128)(2,1)}, f32[8,128]{1,0:T(8,128)S(1)}) custom-call(bf16[4096,2048]{1,0:T(8,128)(2,1)S(1)} %get-tuple-element.13.src), custom_call_target="tpu_custom_call" | custom-call | tf_op jit(solution)/shard_map/pallas_call | solution.py:385
  201.2 6.0 %shard_map.78 = (bf16[2048,4096]{1,0:T(8,128)(2,1)}, f32[8,128]{1,0:T(8,128)S(1)}) custom-call(bf16[2048,4096]{1,0:T(8,128)(2,1)S(1)} %get-tuple-element.15.src), custom_call_target="tpu_custom_call" | custom-call | tf_op jit(solution)/shard_map/pallas_call | solution.py:385
  207.2 0.0 copy-done
  207.2 0.0 copy-done.1
  207.2 17.6 %shard_map.79 = bf16[16,4096]{1,0:T(8,128)(2,1)S(1)} custom-call(f32[128,4096]{1,0:T(8,128)S(1)} %get-tuple-element.11.pacc, f32[1,4096]{1,0:T(1,128)S(1)} %bitcast.6, bf16[16,4096]{1,0:T(8,128)(2,1)S(1)} %copy-done, f32[8,128]{1,0:T(8,128)S(1)} %get-tuple-element.14.up_token, f32[8,128]{1,0:T(8,128)S(1)} %get-tuple-element.16.down_token), custom_call_target="tpu_custom_call" | custom-call | tf_op jit(solution)/shard_map/pallas_call | solution.py:479
  224.8 0.7 copy.9
Async XLA Ops:
  195.2 11.9 %copy-start = (bf16[16,4096]{1,0:T(8,128)(2,1)S(1)}, bf16[16,4096]{1,0:T(8,128)(2,1)}, u32[]{:S(2)}) copy-start(bf16[16,4096]{1,0:T(8,128)(2,1)} %get-tuple-element.12.early) | copy-start | bytes 393220
  195.2 11.9 %copy-start.1 = (f32[4096]{0:T(1024)S(1)}, f32[4096]{0:T(1024)}, u32[]{:S(2)}) copy-start(f32[4096]{0:T(1024)} %param.9) | copy-start | bytes 49156

commit v4 on v3

--- a/solution.py
+++ b/solution.py
@@ -41,8 +41,8 @@
 
 def spread_kernel(
     n_fs, n_tp, w, fused,
-    up_in, down_in, tokens, gain, post, held_up, held_down, pacc, out,
-    stage, dstage, upb, xup, gcol, normed, acc, hid, us, ds_in,
+    up_in, down_in, tokens, gain, post, held_up, held_down, pacc, hid, out,
+    stage, dstage, upb, xup, gcol, normed, acc, us, ds_in,
     xs, xr, ps, pr, ws, wr, ns, nr, ds, dr, vs, vr, *reduce_refs,
 ):
     f, t = lax.axis_index("fs"), lax.axis_index("tp")
@@ -60,9 +60,11 @@
     block_of_f = f // m
     active = lax.rem(lax.rem(block_of_f, 2) + lax.rem(t, 2), 2) == 0
 
+    depth = stage.shape[0]
+
     def load_up(k):
         return pltpu.make_async_copy(
-            up_in.at[:, span(lax.rem(k, m) * n_c + k // m, w)], stage.at[k], us.at[k]
+            up_in.at[:, span(lax.rem(k, m) * n_c + k // m, w)], stage.at[lax.rem(k, depth)], us.at[lax.rem(k, depth)]
         )
 
     def load_down(c):
@@ -74,9 +76,12 @@
     n_s = PARTS if rows % (16 * PARTS) == 0 else 1
     sub = rows // n_s
 
-    def x_copy(k, r):
+    def x_part(k, r):
         at = pl.ds(r * sub, sub)
-        return remote(upb.at[k, at], xup.at[k, at], xs.at[k], xr.at[k, r], {"tp": far})
+        return remote(upb.at[k, at], xup.at[k, at], xs, xr.at[k * n_s + r], {"tp": far})
+
+    def x_copy(k):
+        return remote(upb.at[k], xup.at[k], xs, xr.at[m * (n_s - 1) + k], {"tp": far})
 
     def owner(phase, k):
         return (t if phase == 0 else far) * m + lax.rem(k, m)
@@ -85,27 +90,38 @@
         held = upb if phase == 0 else xup
         to = held_up.at[pl.ds(pl.multiple_of(f * rows + first, size), size), span(k // m, w)]
         return remote(
-            held.at[k, pl.ds(first, size)], to, ps.at[phase, k], pr.at[f, k // m], {"fs": owner(phase, k)}
+            held.at[k, pl.ds(first, size)], to, ps.at[phase], pr.at[f, k // m], {"fs": owner(phase, k)}
         )
 
-    def start_peer(phase, k, r):
+    def start_peer(phase, k, first, size):
         @pl.when(owner(phase, k) != f)
         def _():
-            peer_copy(phase, k, r * sub, sub).start()
-
-    def end_peer(phase, k):
-        @pl.when(owner(phase, k) != f)
-        def _():
-            peer_copy(phase, k, 0, rows).wait_send()
+            peer_copy(phase, k, first, size).start()
+
+    def end_peers(phase):
+        held = upb if phase == 0 else xup
+        own = block_of_f == (t if phase == 0 else far)
+
+        def ended(count):
+            sent = held.at[pl.ds(0, count)]
+            remote(sent, sent, ps.at[phase], ps.at[phase], {"tp": far}).wait_send()
+
+        @pl.when(own)
+        def _():
+            ended(pieces - n_c)
+
+        @pl.when(jnp.logical_not(own))
+        def _():
+            ended(pieces)
 
     def block(c, which):
         return held_down.at[span(c, d_part), span(which, d_width)]
 
     def d_copy(c):
-        return remote(block(c, t), block(c, t), ds.at[c], dr.at[c], {"tp": far})
+        return remote(block(c, t), block(c, t), ds, dr.at[c], {"tp": far})
 
     def d_pass(c, which):
-        return remote(block(c, which), block(c, which), vs.at[c], vr.at[c], {"tp": near})
+        return remote(block(c, which), block(c, which), vs, vr.at[c], {"tp": near})
 
     def column(which):
         return held_down.at[:, span(which, d_width)]
@@ -114,12 +130,11 @@
         return remote(column(which), column(which), ns, nr, {"tp": near})
 
     def share(src, source, c):
-        return remote(src, landed(source, c), ws.at[source, c], wr.at[source, c], {"tp": near})
+        return remote(src, landed(source, c), ws, wr.at[source, c], {"tp": near})
 
     loop(n_fs - 1, lambda i: greet({"fs": lax.rem(f + 1 + i, n_fs)}))
     greet({"tp": far})
     greet({"tp": near})
-    depth = min(DEPTH, pieces)
     loop(depth, lambda k: load_up(k).start())
     for c in range(min(2, n_c)):
         load_down(c).start()
@@ -133,30 +148,37 @@
 
     def convert(k):
         load_up(k).wait()
+        for j in range(0, w, 128):
+            upb[k, :, j : j + 128] = (gcol[...] * stage[lax.rem(k, depth), :, j : j + 128]).astype(upb.dtype)
 
         @pl.when(k + depth < pieces)
         def _():
             load_up(k + depth).start()
 
-        for j in range(0, w, 128):
-            upb[k, :, j : j + 128] = (gcol[...] * stage[k, :, j : j + 128]).astype(upb.dtype)
+    def send_parts(k):
+        for r in range(n_s):
+            x_part(k, r).start()
+        for r in range(n_s):
+            start_peer(0, k, r * sub, sub)
 
     def send(k):
-        for r in range(n_s):
-            x_copy(k, r).start()
-        for r in range(n_s):
-            start_peer(0, k, r)
+        x_copy(k).start()
+        start_peer(0, k, 0, rows)
 
     convert(0)
     pl.semaphore_wait(pltpu.get_barrier_semaphore(), n_fs + 1)
+
+    for k in range(min(m, pieces - 1)):
+        convert(k + 1)
+        send_parts(k)
 
     def convert_and_send(k):
         convert(k)
         send(k - 1)
 
-    lax.fori_loop(1, pieces, lambda k, c: (convert_and_send(k), c)[1], 0)
+    lax.fori_loop(m + 1, pieces, lambda k, c: (convert_and_send(k), c)[1], 0)
     pacc[...] = jnp.zeros_like(pacc)
-    send(pieces - 1)
+    (send if pieces > m else send_parts)(pieces - 1)
 
     def convert_down(c):
         load_down(c).wait()
@@ -166,15 +188,11 @@
         def _():
             load_down(c + 2).start()
 
-    def pass_on(k):
+    def between(k):
         @pl.when(k == max(pieces - 2, 0))
         def _():
             loop(n_c, lambda c: d_copy(c).start())
             to_near(t).start()
-
-        for r in range(n_s):
-            x_copy(k, r).wait_recv()
-            start_peer(1, k, r)
 
         @pl.when(k < n_c)
         def _():
@@ -186,10 +204,22 @@
             for i in range(n_fs):
                 normed[i] = scaled[:, i * rows : (i + 1) * rows]
 
-    loop(pieces, pass_on)
+    def pass_parts(k):
+        for r in range(n_s):
+            x_part(k, r).wait_recv()
+            start_peer(1, k, r * sub, sub)
+        between(k)
+
+    def pass_on(k):
+        x_copy(k).wait_recv()
+        start_peer(1, k, 0, rows)
+        between(k)
+
+    loop(m, pass_parts)
+    lax.fori_loop(m, pieces, lambda k, c: (pass_on(k), c)[1], 0)
 
     def gather(c):
-        remote(block(c, far), block(c, far), ds.at[c], dr.at[c], {"tp": far}).wait_recv()
+        remote(block(c, far), block(c, far), ds, dr.at[c], {"tp": far}).wait_recv()
         d_pass(c, far).start()
         acc[...] = jnp.zeros_like(acc)
 
@@ -215,7 +245,7 @@
 
             @pl.when(jnp.logical_and(active, source != f))
             def _():
-                remote(landed(source, c), landed(source, c), ws.at[source, c], pr.at[source, c], {"tp": near}).wait_recv()
+                remote(landed(source, c), landed(source, c), ws, pr.at[source, c], {"tp": near}).wait_recv()
                 share(landed(source, c), source, c).start()
 
             @pl.when(jnp.logical_not(active))
@@ -253,39 +283,24 @@
     if fused:
         @pl.when(lax.rem(t, 2) == 0)
         def _():
-            reduce_rows(pacc, post, out, lambda s, seg: add_down(last, s * seg, seg), *reduce_refs)
-
-        @pl.when(lax.rem(t, 2) == 1)
-        def _():
-            add_down(last, 0, width)
+            reduce_rows(pacc, post, out, lambda s, seg: add_down(last, s * seg, seg), False, *reduce_refs)
     else:
         add_down(last, 0, width)
         out[...] = jnp.zeros_like(out)
 
-    def ended(i):
-        @pl.when(active)
-        def _():
-            source, c = i // n_c, lax.rem(i, n_c)
-            share(landed(source, c), source, c).wait_send()
-
-    loop(n_fs * n_c, ended)
+    @pl.when(active)
+    def _():
+        remote(held_up, held_up, ws, ws, {"tp": near}).wait_send()
+
     to_near(t).wait_send()
-
-    def ended_down(c):
-        d_copy(c).wait_send()
-        d_pass(c, far).wait_send()
-
-    loop(n_c, ended_down)
-
-    def ended_pieces(k):
-        remote(upb.at[k], xup.at[k], xs.at[k], xr.at[k, 0], {"tp": far}).wait_send()
-        end_peer(0, k)
-        end_peer(1, k)
-
-    loop(pieces, ended_pieces)
-
-
-def reduce_rows(pacc, post, out, compute, sb, land, sb2, land2, fin, ss, rs, ss2, rs2):
+    remote(column(t), column(t), ds, ds, {"tp": far}).wait_send()
+    remote(column(far), column(far), vs, vs, {"tp": near}).wait_send()
+    remote(upb, xup, xs, xs, {"tp": far}).wait_send()
+    end_peers(0)
+    end_peers(1)
+
+
+def reduce_rows(pacc, post, out, compute, waiting, sb, land, sb2, land2, fin, ss, rs, ss2, rs2):
     f = lax.axis_index("fs")
     _, q, n_o, part, seg = sb.shape
     i, o = lax.rem(f, q), f // q
@@ -297,10 +312,10 @@
         return lax.rem(o + d, n_o)
 
     def first_copy(s, d):
-        return remote(sb.at[s, peer(d)], land.at[s, i], ss.at[s, d], rs.at[s, i], {"fs": o * q + peer(d)})
+        return remote(sb.at[s, peer(d)], land.at[s, i], ss, rs.at[s, i], {"fs": o * q + peer(d)})
 
     def second_copy(s, d):
-        return remote(sb2.at[s, across(d)], land2.at[s, o], ss2.at[s, d], rs2.at[s, o], {"fs": across(d) * q + i})
+        return remote(sb2.at[s, across(d)], land2.at[s, o], ss2, rs2.at[s, o], {"fs": across(d) * q + i})
 
     def fill(s):
         for b in range(n_o * q):
@@ -310,8 +325,9 @@
         for d in range(1, q):
             first_copy(s, d).start()
 
-    if compute is None:
+    if waiting:
         for s in range(SEGMENTS):
+            compute(s, seg)
             fill(s)
         pl.semaphore_wait(pltpu.get_barrier_semaphore(), n_o * q - 1)
         for s in range(SEGMENTS):
@@ -324,7 +340,7 @@
 
     for s in range(SEGMENTS):
         for d in range(1, q):
-            remote(land.at[s, peer(d)], land.at[s, peer(d)], ss.at[s, d], rs.at[s, peer(d)], {"fs": f}).wait_recv()
+            remote(land.at[s, peer(d)], land.at[s, peer(d)], ss, rs.at[s, peer(d)], {"fs": f}).wait_recv()
 
         def total(to):
             value = pacc[span(to * q + i, part), s * seg : (s + 1) * seg]
@@ -341,26 +357,33 @@
     for s in range(SEGMENTS):
         value = fin[:, s * seg : (s + 1) * seg]
         for d in range(1, n_o):
-            remote(land2.at[s, across(d)], land2.at[s, across(d)], ss2.at[s, d], rs2.at[s, across(d)], {"fs": f}).wait_recv()
+            remote(land2.at[s, across(d)], land2.at[s, across(d)], ss2, rs2.at[s, across(d)], {"fs": f}).wait_recv()
             value += land2[s, across(d)].astype(jnp.float32)
         fin[:, s * seg : (s + 1) * seg] = value
     summed = fin[...]
     scale = lax.rsqrt(jnp.mean(summed * summed, axis=-1, keepdims=True) + EPS)
     out[...] = (summed * scale * post[...]).astype(out.dtype)
-    for s in range(SEGMENTS):
-        for d in range(1, q):
-            first_copy(s, d).wait_send()
-        for d in range(1, n_o):
-            second_copy(s, d).wait_send()
-
-
-def late_kernel(n_fs, pacc, post, early, up_token, down_token, out, *refs):
+    for buffer, count, sem in ((sb, q - 1, ss), (sb2, n_o - 1, ss2)):
+        sent = buffer.at[:, pl.ds(0, count)]
+        remote(sent, sent, sem, sem, {"fs": f}).wait_send()
+
+
+def late_kernel(n_fs, parts, hidden, held_down, post, early, up_token, down_token, out, pacc, *refs):
     f, t = lax.axis_index("fs"), lax.axis_index("tp")
 
     @pl.when(lax.rem(t, 2) == 1)
     def _():
         loop(n_fs - 1, lambda i: greet({"fs": lax.rem(f + 1 + i, n_fs)}))
-        reduce_rows(pacc, post, out, None, *refs)
+        w = hidden.shape[1]
+        tile = 512
+
+        def add_last(s, seg):
+            for j in range(s * seg, (s + 1) * seg, tile):
+                down = held_down[held_down.shape[0] - w :, j : j + tile]
+                product = jnp.dot(hidden[...], down, preferred_element_type=jnp.float32)
+                pacc[:, j : j + tile] = parts[:, j : j + tile] + product
+
+        reduce_rows(pacc, post, out, add_last, True, *refs)
 
     @pl.when(lax.rem(t, 2) == 0)
     def _():
@@ -441,35 +464,35 @@
         pltpu.VMEM((SEGMENTS, n_o, share, seg), bf16),
         pltpu.VMEM((SEGMENTS, n_o, share, seg), bf16),
         pltpu.VMEM((share, width), f32),
-        dma((SEGMENTS, q)), dma((SEGMENTS, q)),
-        dma((SEGMENTS, n_o)), dma((SEGMENTS, n_o)),
+        dma, dma((SEGMENTS, q)),
+        dma, dma((SEGMENTS, n_o)),
     ]
-    held_up, held_down, parts, early = pl.pallas_call(
+    held_up, held_down, parts, hidden, early = pl.pallas_call(
         functools.partial(spread_kernel, n_fs, n_tp, w, fused),
         out_shape=(
             pltpu.VMEM((n_fs * rows, owned), bf16),
             pltpu.VMEM((d_rows, n_tp * d_cols), bf16),
             pltpu.VMEM((tokens, width), f32),
+            pltpu.VMEM((tokens, w), bf16),
             jax.ShapeDtypeStruct((share, width), bf16),
         ),
         in_specs=[anywhere, anywhere, vmem, vmem, vmem],
-        out_specs=(vmem, vmem, vmem, vmem),
+        out_specs=(vmem, vmem, vmem, vmem, vmem),
         scratch_shapes=[
-            pltpu.VMEM((pieces, rows, w), f32),
+            pltpu.VMEM((min(DEPTH, pieces), rows, w), f32),
             pltpu.VMEM((2, d_rows // n_c, d_cols), f32),
             pltpu.VMEM((pieces, rows, w), bf16),
             pltpu.VMEM((pieces, rows, w), bf16),
             pltpu.VMEM((rows, 128), f32),
             pltpu.VMEM((n_fs, tokens, rows), bf16),
             pltpu.VMEM((tokens, w), f32),
-            pltpu.VMEM((tokens, w), bf16),
-            dma((pieces,)), dma((2,)),
-            dma((pieces,)), dma((pieces, PARTS)),
-            dma((2, pieces)), dma((n_fs, n_c)),
-            dma((n_fs, n_c)), dma((n_fs, n_c)),
+            dma((min(DEPTH, pieces),)), dma((2,)),
+            dma, dma((pieces + m * (PARTS - 1),)),
+            dma((2,)), dma((n_fs, n_c)),
+            dma, dma((n_fs, n_c)),
             dma, dma,
-            dma((n_c,)), dma((n_c,)),
-            dma((n_c,)), dma((n_c,)),
+            dma, dma((n_c,)),
+            dma, dma((n_c,)),
         ] + (reduce_scratch if fused else []),
         compiler_params=pltpu.CompilerParams(collective_id=0, has_side_effects=True, vmem_limit_bytes=30500000),
     )(trained_up, trained_down, prompt_tokens[0], pre_gain[None], post_gain[None])
@@ -479,11 +502,11 @@
         layer_out = pl.pallas_call(
             functools.partial(late_kernel, n_fs),
             out_shape=jax.ShapeDtypeStruct((share, width), bf16),
-            in_specs=[vmem, vmem, vmem, anywhere, anywhere],
+            in_specs=[vmem, vmem, vmem, vmem, vmem, anywhere, anywhere],
             out_specs=vmem,
-            scratch_shapes=reduce_scratch,
+            scratch_shapes=[pltpu.VMEM((tokens, width), f32)] + reduce_scratch,
             compiler_params=pltpu.CompilerParams(collective_id=1, has_side_effects=True, vmem_limit_bytes=16000000),
-        )(parts, post_gain[None], early, up_token, down_token)
+        )(parts, hidden, held_down, post_gain[None], early, up_token, down_token)
         return (layer_out[None], sampler_up, sampler_down)
 
     layer_out = pl.pallas_call(

time: 227 us -> 222 us (0.978)
  Pallas kernels: 224 us -> 219 us
    pallas_call x1, Pallas kernels: 195 us -> 192 us  [on_device(): pl.pallas_call(functools.partial(spread_kernel, n_fs, n_tp, w, fused), ou...]
where the time goes in v4:
time: 222 us; the launch traced here: 221 us
  Pallas kernels  219 us (99%)
    pallas_call x1, Pallas kernels, on_device(): pl.pallas_call(functools.partial(spread_kernel, n_fs, n_tp, w, fused), ou...  192 us
    pallas_call x1, Pallas kernels, on_device(): pl.pallas_call(functools.partial(late_kernel, n_fs), out_shape=jax.ShapeD...  15.7 us
    pallas_call x2, Pallas kernels, store(): pl.pallas_call(store_kernel, out_shape=(jax.ShapeDtypeStruct(array.shape,...  11.9 us

profile of v4, /device:TPU:13, one launch (start us, length us, event | category | flops | bytes accessed | tf_op | source)
XLA Modules:
  0.0 220.7 jit_solution(14483770700731561119)
XLA Ops:
  0.6 191.7 %shard_map.76 = (bf16[4096,2048]{1,0:T(8,128)(2,1)S(1)}, bf16[2048,4096]{1,0:T(8,128)(2,1)S(1)}, f32[128,4096]{1,0:T(8,128)S(1)}, bf16[128,256]{1,0:T(8,128)(2,1)S(1)}, bf16[16,4096]{1,0:T(8,128)(2,1)}) custom-call(f32[512,4096]{1,0:T(8,128)} %up_in.1, f32[2048,1024]{1,0:T(8,128)} %down_in.1, bf16[128,4096]{1,0:T(8,128)(2,1)} %bitcast.7, f32[1,512]{1,0:T(1,128)} %bitcast.8, ...), custom_call_target="tpu_custom_call" | custom-call | tf_op jit(solution)/shard_map/pallas_call | solution.py:470
  192.4 0.0 copy-start
  192.4 0.0 copy-start.1
  192.4 6.0 %shard_map.77 = (bf16[4096,2048]{1,0:T(8,128)(2,1)}, f32[8,128]{1,0:T(8,128)S(1)}) custom-call(bf16[4096,2048]{1,0:T(8,128)(2,1)S(1)} %get-tuple-element.16.src), custom_call_target="tpu_custom_call" | custom-call | tf_op jit(solution)/shard_map/pallas_call | solution.py:408
  198.4 6.0 %shard_map.78 = (bf16[2048,4096]{1,0:T(8,128)(2,1)}, f32[8,128]{1,0:T(8,128)S(1)}) custom-call(bf16[2048,4096]{1,0:T(8,128)(2,1)S(1)} %get-tuple-element.14.src.held_down), custom_call_target="tpu_custom_call" | custom-call | tf_op jit(solution)/shard_map/pallas_call | solution.py:408
  204.3 0.0 copy-done
  204.3 0.0 copy-done.1
  204.3 15.7 %shard_map.79 = bf16[16,4096]{1,0:T(8,128)(2,1)S(1)} custom-call(f32[128,4096]{1,0:T(8,128)S(1)} %get-tuple-element.12.parts, bf16[128,256]{1,0:T(8,128)(2,1)S(1)} %get-tuple-element.13.hidden, bf16[2048,4096]{1,0:T(8,128)(2,1)S(1)} %get-tuple-element.14.src.held_down, f32[1,4096]{1,0:T(1,128)S(1)} %bitcast.6, bf16[16,4096]{1,0:T(8,128)(2,1)S(1)} %copy-done, ...), custom_call_target="tpu_custom_call" | custom-call | tf_op jit(solution)/shard_map/pallas_call | solution.py:502
  220.1 0.7 copy.9
Async XLA Ops:
  192.4 11.9 %copy-start = (bf16[16,4096]{1,0:T(8,128)(2,1)S(1)}, bf16[16,4096]{1,0:T(8,128)(2,1)}, u32[]{:S(2)}) copy-start(bf16[16,4096]{1,0:T(8,128)(2,1)} %get-tuple-element.15.early) | copy-start | bytes 393220
  192.4 11.9 %copy-start.1 = (f32[4096]{0:T(1024)S(1)}, f32[4096]{0:T(1024)}, u32[]{:S(2)}) copy-start(f32[4096]{0:T(1024)} %param.9) | copy-start | bytes 49156

commit v5 on v4

--- a/solution.py
+++ b/solution.py
@@ -43,7 +43,7 @@
     n_fs, n_tp, w, fused,
     up_in, down_in, tokens, gain, post, held_up, held_down, pacc, hid, out,
     stage, dstage, upb, xup, gcol, normed, acc, us, ds_in,
-    xs, xr, ps, pr, ws, wr, ns, nr, ds, dr, vs, vr, *reduce_refs,
+    xs, xr, ps, pr, prf, ws, wr, wrf, ns, nr, ds, dr, vs, vr, *reduce_refs,
 ):
     f, t = lax.axis_index("fs"), lax.axis_index("tp")
     far = lax.rem(t + n_tp // 2, n_tp)
@@ -73,7 +73,10 @@
     def landed(source, c):
         return held_up.at[span(source, rows), span(c, w)]
 
+    half = n_fs // 2
     n_s = PARTS if rows % (16 * PARTS) == 0 else 1
+    fine = n_s > 1 and n_c > 2
+    closing = pieces - m if fine else pieces
     sub = rows // n_s
 
     def x_part(k, r):
@@ -86,17 +89,19 @@
     def owner(phase, k):
         return (t if phase == 0 else far) * m + lax.rem(k, m)
 
-    def peer_copy(phase, k, first, size):
-        held = upb if phase == 0 else xup
-        to = held_up.at[pl.ds(pl.multiple_of(f * rows + first, size), size), span(k // m, w)]
-        return remote(
-            held.at[k, pl.ds(first, size)], to, ps.at[phase], pr.at[f, k // m], {"fs": owner(phase, k)}
-        )
-
-    def start_peer(phase, k, first, size):
-        @pl.when(owner(phase, k) != f)
-        def _():
-            peer_copy(phase, k, first, size).start()
+    def landed_part(source, c, r):
+        return held_up.at[pl.ds(pl.multiple_of(source * rows + r * sub, sub), sub), span(c, w)]
+
+    def start_peer(phase, k, first, size, sem=None):
+        to = owner(phase, k)
+        held = (upb if phase == 0 else xup).at[k, pl.ds(first, size)]
+        at = held_up.at[pl.ds(pl.multiple_of(f * rows + first, size), size), span(k // m, w)]
+        if sem is None:
+            sem = pr.at[lax.rem(f // half + to // half, 2), k // m]
+
+        @pl.when(to != f)
+        def _():
+            remote(held, at, ps.at[phase], sem, {"fs": to}).start()
 
     def end_peers(phase):
         held = upb if phase == 0 else xup
@@ -128,9 +133,6 @@
 
     def to_near(which):
         return remote(column(which), column(which), ns, nr, {"tp": near})
-
-    def share(src, source, c):
-        return remote(src, landed(source, c), ws, wr.at[source, c], {"tp": near})
 
     loop(n_fs - 1, lambda i: greet({"fs": lax.rem(f + 1 + i, n_fs)}))
     greet({"tp": far})
@@ -172,13 +174,21 @@
         convert(k + 1)
         send_parts(k)
 
+    def send_closing(k):
+        x_copy(k).start()
+        for r in range(n_s):
+            start_peer(0, k, r * sub, sub, prf.at[f, r])
+
     def convert_and_send(k):
         convert(k)
         send(k - 1)
 
-    lax.fori_loop(m + 1, pieces, lambda k, c: (convert_and_send(k), c)[1], 0)
+    lax.fori_loop(m + 1, closing + 1 if fine else pieces, lambda k, c: (convert_and_send(k), c)[1], 0)
+    for k in range(closing, pieces - 1):
+        convert(k + 1)
+        send_closing(k)
     pacc[...] = jnp.zeros_like(pacc)
-    (send if pieces > m else send_parts)(pieces - 1)
+    (send_closing if fine else send if pieces > m else send_parts)(pieces - 1)
 
     def convert_down(c):
         load_down(c).wait()
@@ -215,48 +225,101 @@
         start_peer(1, k, 0, rows)
         between(k)
 
+    def pass_closing(k):
+        x_copy(k).wait_recv()
+        for r in range(n_s):
+            start_peer(1, k, r * sub, sub, prf.at[f, r])
+        between(k)
+
     loop(m, pass_parts)
-    lax.fori_loop(m, pieces, lambda k, c: (pass_on(k), c)[1], 0)
-
-    def gather(c):
+    lax.fori_loop(m, closing, lambda k, c: (pass_on(k), c)[1], 0)
+    lax.fori_loop(closing, pieces, lambda k, c: (pass_closing(k), c)[1], 0)
+
+    def gather(c, final):
         remote(block(c, far), block(c, far), ds, dr.at[c], {"tp": far}).wait_recv()
         d_pass(c, far).start()
         acc[...] = jnp.zeros_like(acc)
-
-        def one(step):
-            half = n_fs // 2
-            side = lax.rem(f // half + step // half, 2)
-            source = side * half + lax.rem(f + step, half)
-
-            def keep_own(held):
-                k = c * m + lax.rem(f, m)
-                share(held.at[k], source, c).start()
-                held_up[span(source, rows), span(c, w)] = held[k]
-
-            @pl.when(jnp.logical_and(active, source == f))
-            def _():
-                @pl.when(block_of_f == t)
-                def _():
-                    keep_own(upb)
-
-                @pl.when(block_of_f != t)
-                def _():
-                    keep_own(xup)
-
-            @pl.when(jnp.logical_and(active, source != f))
-            def _():
-                remote(landed(source, c), landed(source, c), ws, pr.at[source, c], {"tp": near}).wait_recv()
-                share(landed(source, c), source, c).start()
-
-            @pl.when(jnp.logical_not(active))
-            def _():
-                share(landed(source, c), source, c).wait_recv()
-
+        mine = f // half
+
+        def source_at(side, step):
+            return lax.rem(mine + side, 2) * half + lax.rem(f + step, half)
+
+        def rows_at(first, count):
+            return held_up.at[pl.ds(pl.multiple_of(first * rows, rows), count * rows), span(c, w)]
+
+        def side_rows(side):
+            return rows_at(lax.rem(mine + side, 2) * half, half)
+
+        def share(src, to, sem):
+            return remote(src, to, ws, sem, {"tp": near})
+
+        def share_sem(side, source):
+            return wrf.at[source] if final else wr.at[side, c]
+
+        def keep_own(held):
+            k = c * m + lax.rem(f, m)
+            share(held.at[k], rows_at(f, 1), share_sem(0, f)).start()
+            held_up[span(f, rows), span(c, w)] = held[k]
+
+        @pl.when(jnp.logical_and(active, block_of_f == t))
+        def _():
+            keep_own(upb)
+
+        @pl.when(jnp.logical_and(active, block_of_f != t))
+        def _():
+            keep_own(xup)
+
+        def pass_part(side, i):
+            source, r = source_at(side, lax.rem(i, half)), i // half
+            part = landed_part(source, c, r)
+            share(part, part, prf.at[source, r]).wait_recv()
+            share(part, part, wrf.at[source]).start()
+
+        def add_up(source):
             acc[...] += jnp.dot(
                 normed[source], held_up[span(source, rows), span(c, w)], preferred_element_type=jnp.float32
             )
 
-        loop(n_fs, one)
+        for side in range(2):
+            @pl.when(active)
+            def _():
+                if final:
+                    def one(i):
+                        @pl.when(jnp.logical_or(side > 0, lax.rem(i, half) > 0))
+                        def _():
+                            pass_part(side, i)
+
+                    loop(half * n_s, one)
+                elif side == 0:
+                    others = rows_at(0, half - 1)
+                    share(others, others, pr.at[side, c]).wait_recv()
+
+                    def one(i):
+                        at = rows_at(source_at(side, i + 1), 1)
+                        share(at, at, wr.at[side, c]).start()
+
+                    loop(half - 1, one)
+                else:
+                    at = side_rows(side)
+                    share(at, at, pr.at[side, c]).wait_recv()
+                    share(at, at, wr.at[side, c]).start()
+
+            if not final:
+                @pl.when(jnp.logical_not(active))
+                def _():
+                    share(side_rows(side), side_rows(side), wr.at[side, c]).wait_recv()
+
+            def close_one(step):
+                source = source_at(side, step)
+                if final:
+                    @pl.when(jnp.logical_not(active))
+                    def _():
+                        share(rows_at(source, 1), rows_at(source, 1), wrf.at[source]).wait_recv()
+
+                add_up(source)
+
+            loop(half, close_one)
+
         hid[...] = jnp.square(jnp.maximum(acc[...], 0.0)).astype(jnp.bfloat16)
         d_pass(c, near_far).wait_recv()
 
@@ -274,12 +337,12 @@
         loop(count // tile, one)
 
     def whole_chunk(c):
-        gather(c)
+        gather(c, False)
         add_down(c, 0, width)
 
     last = n_c - 1
     loop(last, whole_chunk)
-    gather(last)
+    gather(last, fine)
     if fused:
         @pl.when(lax.rem(t, 2) == 0)
         def _():
@@ -312,10 +375,12 @@
         return lax.rem(o + d, n_o)
 
     def first_copy(s, d):
-        return remote(sb.at[s, peer(d)], land.at[s, i], ss, rs.at[s, i], {"fs": o * q + peer(d)})
+        return remote(sb.at[s, peer(d)], land.at[s, i], ss, rs.at[s], {"fs": o * q + peer(d)})
 
     def second_copy(s, d):
-        return remote(sb2.at[s, across(d)], land2.at[s, o], ss2, rs2.at[s, o], {"fs": across(d) * q + i})
+        return remote(sb2.at[s, across(d)], land2.at[s, o], ss2, rs2.at[s], {"fs": across(d) * q + i})
+
+    ready = SEGMENTS // 2
 
     def fill(s):
         for b in range(n_o * q):
@@ -329,9 +394,12 @@
         for s in range(SEGMENTS):
             compute(s, seg)
             fill(s)
-        pl.semaphore_wait(pltpu.get_barrier_semaphore(), n_o * q - 1)
-        for s in range(SEGMENTS):
-            send(s)
+            if s == ready:
+                pl.semaphore_wait(pltpu.get_barrier_semaphore(), n_o * q - 1)
+                for r in range(s):
+                    send(r)
+            if s >= ready:
+                send(s)
     else:
         for s in range(SEGMENTS):
             compute(s, seg)
@@ -339,8 +407,8 @@
             send(s)
 
     for s in range(SEGMENTS):
-        for d in range(1, q):
-            remote(land.at[s, peer(d)], land.at[s, peer(d)], ss, rs.at[s, peer(d)], {"fs": f}).wait_recv()
+        arrived = land.at[s, pl.ds(0, q - 1)]
+        remote(arrived, arrived, ss, rs.at[s], {"fs": f}).wait_recv()
 
         def total(to):
             value = pacc[span(to * q + i, part), s * seg : (s + 1) * seg]
@@ -356,8 +424,9 @@
 
     for s in range(SEGMENTS):
         value = fin[:, s * seg : (s + 1) * seg]
+        arrived = land2.at[s, pl.ds(0, n_o - 1)]
+        remote(arrived, arrived, ss2, rs2.at[s], {"fs": f}).wait_recv()
         for d in range(1, n_o):
-            remote(land2.at[s, across(d)], land2.at[s, across(d)], ss2, rs2.at[s, across(d)], {"fs": f}).wait_recv()
             value += land2[s, across(d)].astype(jnp.float32)
         fin[:, s * seg : (s + 1) * seg] = value
     summed = fin[...]
@@ -464,8 +533,8 @@
         pltpu.VMEM((SEGMENTS, n_o, share, seg), bf16),
         pltpu.VMEM((SEGMENTS, n_o, share, seg), bf16),
         pltpu.VMEM((share, width), f32),
-        dma, dma((SEGMENTS, q)),
-        dma, dma((SEGMENTS, n_o)),
+        dma, dma((SEGMENTS,)),
+        dma, dma((SEGMENTS,)),
     ]
     held_up, held_down, parts, hidden, early = pl.pallas_call(
         functools.partial(spread_kernel, n_fs, n_tp, w, fused),
@@ -488,8 +557,8 @@
             pltpu.VMEM((tokens, w), f32),
             dma((min(DEPTH, pieces),)), dma((2,)),
             dma, dma((pieces + m * (PARTS - 1),)),
-            dma((2,)), dma((n_fs, n_c)),
-            dma, dma((n_fs, n_c)),
+            dma((2,)), dma((2, n_c)), dma((n_fs, PARTS)),
+            dma, dma((2, n_c)), dma((n_fs,)),
             dma, dma,
             dma, dma((n_c,)),
             dma, dma((n_c,)),

time: 222 us -> 221 us (level)
  no operation moved by 1% of the time
where the time goes in v5:
time: 221 us; the launch traced here: 220 us
  Pallas kernels  218 us (99%)
    pallas_call x1, Pallas kernels, on_device(): pl.pallas_call(functools.partial(spread_kernel, n_fs, n_tp, w, fused), ou...  191 us
    pallas_call x1, Pallas kernels, on_device(): pl.pallas_call(functools.partial(late_kernel, n_fs), out_shape=jax.ShapeD...  15.3 us
    pallas_call x2, Pallas kernels, store(): pl.pallas_call(store_kernel, out_shape=(jax.ShapeDtypeStruct(array.shape,...  11.9 us

profile of v5, /device:TPU:13, one launch (start us, length us, event | category | flops | bytes accessed | tf_op | source)
XLA Modules:
  0.0 219.7 jit_solution(13916056580927621156)
XLA Ops:
  0.6 191.1 %shard_map.76 = (bf16[4096,2048]{1,0:T(8,128)(2,1)S(1)}, bf16[2048,4096]{1,0:T(8,128)(2,1)S(1)}, f32[128,4096]{1,0:T(8,128)S(1)}, bf16[128,256]{1,0:T(8,128)(2,1)S(1)}, bf16[16,4096]{1,0:T(8,128)(2,1)}) custom-call(f32[512,4096]{1,0:T(8,128)} %up_in.1, f32[2048,1024]{1,0:T(8,128)} %down_in.1, bf16[128,4096]{1,0:T(8,128)(2,1)} %bitcast.7, f32[1,512]{1,0:T(1,128)} %bitcast.8, ...), custom_call_target="tpu_custom_call" | custom-call | tf_op jit(solution)/shard_map/pallas_call | solution.py:539
  191.7 0.0 copy-start
  191.7 0.0 copy-start.1
  191.8 6.0 %shard_map.77 = (bf16[4096,2048]{1,0:T(8,128)(2,1)}, f32[8,128]{1,0:T(8,128)S(1)}) custom-call(bf16[4096,2048]{1,0:T(8,128)(2,1)S(1)} %get-tuple-element.16.src), custom_call_target="tpu_custom_call" | custom-call | tf_op jit(solution)/shard_map/pallas_call | solution.py:477
  197.7 6.0 %shard_map.78 = (bf16[2048,4096]{1,0:T(8,128)(2,1)}, f32[8,128]{1,0:T(8,128)S(1)}) custom-call(bf16[2048,4096]{1,0:T(8,128)(2,1)S(1)} %get-tuple-element.14.src.held_down), custom_call_target="tpu_custom_call" | custom-call | tf_op jit(solution)/shard_map/pallas_call | solution.py:477
  203.7 0.0 copy-done
  203.7 0.0 copy-done.1
  203.7 15.3 %shard_map.79 = bf16[16,4096]{1,0:T(8,128)(2,1)S(1)} custom-call(f32[128,4096]{1,0:T(8,128)S(1)} %get-tuple-element.12.parts, bf16[128,256]{1,0:T(8,128)(2,1)S(1)} %get-tuple-element.13.hidden, bf16[2048,4096]{1,0:T(8,128)(2,1)S(1)} %get-tuple-element.14.src.held_down, f32[1,4096]{1,0:T(1,128)S(1)} %bitcast.6, bf16[16,4096]{1,0:T(8,128)(2,1)S(1)} %copy-done, ...), custom_call_target="tpu_custom_call" | custom-call | tf_op jit(solution)/shard_map/pallas_call | solution.py:571
  219.0 0.7 copy.9
Async XLA Ops:
  191.7 11.9 %copy-start = (bf16[16,4096]{1,0:T(8,128)(2,1)S(1)}, bf16[16,4096]{1,0:T(8,128)(2,1)}, u32[]{:S(2)}) copy-start(bf16[16,4096]{1,0:T(8,128)(2,1)} %get-tuple-element.15.early) | copy-start | bytes 393220
  191.7 11.9 %copy-start.1 = (f32[4096]{0:T(1024)S(1)}, f32[4096]{0:T(1024)}, u32[]{:S(2)}) copy-start(f32[4096]{0:T(1024)} %param.9) | copy-start | bytes 49156

commit v6 on v5

--- a/solution.py
+++ b/solution.py
@@ -236,8 +236,12 @@
     lax.fori_loop(closing, pieces, lambda k, c: (pass_closing(k), c)[1], 0)
 
     def gather(c, final):
-        remote(block(c, far), block(c, far), ds, dr.at[c], {"tp": far}).wait_recv()
-        d_pass(c, far).start()
+        def pass_down():
+            remote(block(c, far), block(c, far), ds, dr.at[c], {"tp": far}).wait_recv()
+            d_pass(c, far).start()
+
+        if not final:
+            pass_down()
         acc[...] = jnp.zeros_like(acc)
         mine = f // half
 
@@ -281,6 +285,9 @@
             )
 
         for side in range(2):
+            if final and side == 1:
+                pass_down()
+
             @pl.when(active)
             def _():
                 if final:
@@ -380,7 +387,7 @@
     def second_copy(s, d):
         return remote(sb2.at[s, across(d)], land2.at[s, o], ss2, rs2.at[s], {"fs": across(d) * q + i})
 
-    ready = SEGMENTS // 2
+    ready = SEGMENTS // 4
 
     def fill(s):
         for b in range(n_o * q):
@@ -395,7 +402,7 @@
             compute(s, seg)
             fill(s)
             if s == ready:
-                pl.semaphore_wait(pltpu.get_barrier_semaphore(), n_o * q - 1)
+                pl.semaphore_wait(pltpu.get_barrier_semaphore(), q - 1 + n_o - 1)
                 for r in range(s):
                     send(r)
             if s >= ready:
@@ -442,7 +449,12 @@
 
     @pl.when(lax.rem(t, 2) == 1)
     def _():
-        loop(n_fs - 1, lambda i: greet({"fs": lax.rem(f + 1 + i, n_fs)}))
+        _, q, n_o, _, _ = refs[0].shape
+        i, o = lax.rem(f, q), f // q
+        for d in range(1, q):
+            greet({"fs": o * q + lax.rem(i + d, q)})
+        for d in range(1, n_o):
+            greet({"fs": lax.rem(o + d, n_o) * q + i})
         w = hidden.shape[1]
         tile = 512
 

time: 221 us -> 221 us (level)
  no operation moved by 1% of the time
where the time goes in v6:
time: 221 us; the launch traced here: 219 us
  Pallas kernels  218 us (99%)
    pallas_call x1, Pallas kernels, on_device(): pl.pallas_call(functools.partial(spread_kernel, n_fs, n_tp, w, fused), ou...  190 us
    pallas_call x1, Pallas kernels, on_device(): pl.pallas_call(functools.partial(late_kernel, n_fs), out_shape=jax.ShapeD...  16.4 us
    pallas_call x2, Pallas kernels, store(): pl.pallas_call(store_kernel, out_shape=(jax.ShapeDtypeStruct(array.shape,...  11.9 us

profile of v6, /device:TPU:13, one launch (start us, length us, event | category | flops | bytes accessed | tf_op | source)
XLA Modules:
  0.0 219.3 jit_solution(3639630986534087773)
XLA Ops:
  0.6 189.6 %shard_map.76 = (bf16[4096,2048]{1,0:T(8,128)(2,1)S(1)}, bf16[2048,4096]{1,0:T(8,128)(2,1)S(1)}, f32[128,4096]{1,0:T(8,128)S(1)}, bf16[128,256]{1,0:T(8,128)(2,1)S(1)}, bf16[16,4096]{1,0:T(8,128)(2,1)}) custom-call(f32[512,4096]{1,0:T(8,128)} %up_in.1, f32[2048,1024]{1,0:T(8,128)} %down_in.1, bf16[128,4096]{1,0:T(8,128)(2,1)} %bitcast.7, f32[1,512]{1,0:T(1,128)} %bitcast.8, ...), custom_call_target="tpu_custom_call" | custom-call | tf_op jit(solution)/shard_map/pallas_call | solution.py:551
  190.2 0.0 copy-start
  190.2 0.0 copy-start.1
  190.3 6.0 %shard_map.77 = (bf16[4096,2048]{1,0:T(8,128)(2,1)}, f32[8,128]{1,0:T(8,128)S(1)}) custom-call(bf16[4096,2048]{1,0:T(8,128)(2,1)S(1)} %get-tuple-element.16.src), custom_call_target="tpu_custom_call" | custom-call | tf_op jit(solution)/shard_map/pallas_call | solution.py:489
  196.2 6.0 %shard_map.78 = (bf16[2048,4096]{1,0:T(8,128)(2,1)}, f32[8,128]{1,0:T(8,128)S(1)}) custom-call(bf16[2048,4096]{1,0:T(8,128)(2,1)S(1)} %get-tuple-element.14.src.held_down), custom_call_target="tpu_custom_call" | custom-call | tf_op jit(solution)/shard_map/pallas_call | solution.py:489
  202.2 0.0 copy-done
  202.2 0.0 copy-done.1
  202.2 16.4 %shard_map.79 = bf16[16,4096]{1,0:T(8,128)(2,1)S(1)} custom-call(f32[128,4096]{1,0:T(8,128)S(1)} %get-tuple-element.12.parts, bf16[128,256]{1,0:T(8,128)(2,1)S(1)} %get-tuple-element.13.hidden, bf16[2048,4096]{1,0:T(8,128)(2,1)S(1)} %get-tuple-element.14.src.held_down, f32[1,4096]{1,0:T(1,128)S(1)} %bitcast.6, bf16[16,4096]{1,0:T(8,128)(2,1)S(1)} %copy-done, ...), custom_call_target="tpu_custom_call" | custom-call | tf_op jit(solution)/shard_map/pallas_call | solution.py:583
  218.6 0.7 copy.9
Async XLA Ops:
  190.2 11.9 %copy-start = (bf16[16,4096]{1,0:T(8,128)(2,1)S(1)}, bf16[16,4096]{1,0:T(8,128)(2,1)}, u32[]{:S(2)}) copy-start(bf16[16,4096]{1,0:T(8,128)(2,1)} %get-tuple-element.15.early) | copy-start | bytes 393220
  190.2 11.9 %copy-start.1 = (f32[4096]{0:T(1024)S(1)}, f32[4096]{0:T(1024)}, u32[]{:S(2)}) copy-start(f32[4096]{0:T(1024)} %param.9) | copy-start | bytes 49156

commit v7 on v5

--- a/solution.py
+++ b/solution.py
@@ -10,8 +10,8 @@
 MESH = pl.DeviceIdType.MESH
 EPS = 1e-06
 CHUNK = 256
-SEGMENTS = 4
-GROUP = 4
+SEGMENTS = 8
+GROUP = 2
 STORES = 4
 PARTS = 4
 DEPTH = 4
@@ -236,8 +236,12 @@
     lax.fori_loop(closing, pieces, lambda k, c: (pass_closing(k), c)[1], 0)
 
     def gather(c, final):
-        remote(block(c, far), block(c, far), ds, dr.at[c], {"tp": far}).wait_recv()
-        d_pass(c, far).start()
+        def pass_down():
+            remote(block(c, far), block(c, far), ds, dr.at[c], {"tp": far}).wait_recv()
+            d_pass(c, far).start()
+
+        if not final:
+            pass_down()
         acc[...] = jnp.zeros_like(acc)
         mine = f // half
 
@@ -281,6 +285,9 @@
             )
 
         for side in range(2):
+            if final and side == 1:
+                pass_down()
+
             @pl.when(active)
             def _():
                 if final:

time: 221 us -> 221 us (level)
  no operation moved by 1% of the time
where the time goes in v7:
time: 221 us; the launch traced here: 219 us
  Pallas kernels  217 us (98%)
    pallas_call x1, Pallas kernels, on_device(): pl.pallas_call(functools.partial(spread_kernel, n_fs, n_tp, w, fused), ou...  190 us
    pallas_call x1, Pallas kernels, on_device(): pl.pallas_call(functools.partial(late_kernel, n_fs), out_shape=jax.ShapeD...  15.8 us
    pallas_call x2, Pallas kernels, store(): pl.pallas_call(store_kernel, out_shape=(jax.ShapeDtypeStruct(array.shape,...  11.9 us

profile of v7, /device:TPU:13, one launch (start us, length us, event | category | flops | bytes accessed | tf_op | source)
XLA Modules:
  0.0 218.7 jit_solution(5234489001842577871)
XLA Ops:
  0.6 189.7 %shard_map.76 = (bf16[4096,2048]{1,0:T(8,128)(2,1)S(1)}, bf16[2048,4096]{1,0:T(8,128)(2,1)S(1)}, f32[128,4096]{1,0:T(8,128)S(1)}, bf16[128,256]{1,0:T(8,128)(2,1)S(1)}, bf16[16,4096]{1,0:T(8,128)(2,1)}) custom-call(f32[512,4096]{1,0:T(8,128)} %up_in.1, f32[2048,1024]{1,0:T(8,128)} %down_in.1, bf16[128,4096]{1,0:T(8,128)(2,1)} %bitcast.7, f32[1,512]{1,0:T(1,128)} %bitcast.8, ...), custom_call_target="tpu_custom_call" | custom-call | tf_op jit(solution)/shard_map/pallas_call | solution.py:546
  190.3 0.0 copy-start
  190.3 0.0 copy-start.1
  190.3 6.0 %shard_map.77 = (bf16[4096,2048]{1,0:T(8,128)(2,1)}, f32[8,128]{1,0:T(8,128)S(1)}) custom-call(bf16[4096,2048]{1,0:T(8,128)(2,1)S(1)} %get-tuple-element.16.src), custom_call_target="tpu_custom_call" | custom-call | tf_op jit(solution)/shard_map/pallas_call | solution.py:484
  196.3 6.0 %shard_map.78 = (bf16[2048,4096]{1,0:T(8,128)(2,1)}, f32[8,128]{1,0:T(8,128)S(1)}) custom-call(bf16[2048,4096]{1,0:T(8,128)(2,1)S(1)} %get-tuple-element.14.src.held_down), custom_call_target="tpu_custom_call" | custom-call | tf_op jit(solution)/shard_map/pallas_call | solution.py:484
  202.2 0.0 copy-done
  202.3 0.0 copy-done.1
  202.3 15.8 %shard_map.79 = bf16[16,4096]{1,0:T(8,128)(2,1)S(1)} custom-call(f32[128,4096]{1,0:T(8,128)S(1)} %get-tuple-element.12.parts, bf16[128,256]{1,0:T(8,128)(2,1)S(1)} %get-tuple-element.13.hidden, bf16[2048,4096]{1,0:T(8,128)(2,1)S(1)} %get-tuple-element.14.src.held_down, f32[1,4096]{1,0:T(1,128)S(1)} %bitcast.6, bf16[16,4096]{1,0:T(8,128)(2,1)S(1)} %copy-done, ...), custom_call_target="tpu_custom_call" | custom-call | tf_op jit(solution)/shard_map/pallas_call | solution.py:578
  218.1 0.7 copy.9
Async XLA Ops:
  190.3 11.9 %copy-start = (bf16[16,4096]{1,0:T(8,128)(2,1)S(1)}, bf16[16,4096]{1,0:T(8,128)(2,1)}, u32[]{:S(2)}) copy-start(bf16[16,4096]{1,0:T(8,128)(2,1)} %get-tuple-element.15.early) | copy-start | bytes 393220
  190.3 11.9 %copy-start.1 = (f32[4096]{0:T(1024)S(1)}, f32[4096]{0:T(1024)}, u32[]{:S(2)}) copy-start(f32[4096]{0:T(1024)} %param.9) | copy-start | bytes 49156
